TPU v7x, 256 devices: a 4x2x16 block of a 4x16x16 slice. The times are simulated.
256 devices in a mesh: grp: 2 (over y), sp: 16 (over z), fs: 4 (over x), tp: 2 (over core).
Axes of the slice: x: 4, y: 2, z: 16, core: 2. Of those that a mesh axis runs over, the one named last changes fastest.
The devices are a block of a 4x16x16 slice.
Arguments:
- tokens: bfloat16 [8, 4096, 2048], P(('grp', 'fs'), 'sp', 'tp'), parts along dimension 0, may hold values from -6 to 6
- input_norm_gain: float32 [2048], replicated, may hold values from 0.1 to 1.9
- query_weight: bfloat16 [2048, 1024], P('sp', 'tp'), may hold values from -0.125 to 0.125
- key_weight: bfloat16 [2048, 1024], P('sp', 'tp'), may hold values from -0.125 to 0.125
- value_weight: bfloat16 [2048, 1024], P('sp', 'tp'), may hold values from -0.125 to 0.125
- decay_gate_weight: bfloat16 [2048, 8], replicated, may hold values from -0.125 to 0.125
- write_strength_weight: bfloat16 [2048, 8], replicated, may hold values from -0.125 to 0.125
- up_weight: bfloat16 [2048, 1024], P('sp', 'tp'), may hold values from -0.125 to 0.125
- gate_half_weight: bfloat16 [2048, 1024], P('sp', 'tp'), may hold values from -0.125 to 0.125
- log_decay_rate: float32 [8], replicated, may hold values from -30 to 0
- write_strength_bias: float32 [8], replicated, may hold values from -7 to 1
- decay_spike_added: float32 [8, 4096, 8], P(('grp', 'fs'), 'sp', 'tp'), parts along dimension 0, may hold values from -2 to 0
- starting_state: float32 [8, 8, 128, 128], P(('grp', 'fs'), 'tp'), parts along dimension 0, may hold values from -4 to 4
- head_norm_gain: float32 [128], replicated, may hold values from 0.1 to 1.9
- convolution_kernel: float32 [31, 1024], replicated, may hold values from -4 to 4
- channel_norm_gain: float32 [1024], replicated, may hold values from 0.1 to 1.9
- delta_output_rows: bfloat16 [1024, 2048], P('tp', 'sp'), may hold values from -0.125 to 0.125
- convolution_output_rows: bfloat16 [1024, 2048], P('tp', 'sp'), may hold values from -0.125 to 0.125
Outputs:
- mixed: bfloat16 [8, 4096, 2048], P(('grp', 'fs'), 'sp', 'tp'), parts along dimension 0
There are 2 independent parts, one for each index of `grp`. A program takes and returns all parts, laid end to end along the dimension named above; an argument that names none is the same for every part. Nothing has to cross between parts.
All inputs are finite; a program needn't handle non-finite values.
Results may differ from a plain program's by a relative error of at most 0.01.
Values may be sent and summed in bfloat16 or wider, within the bound.
A program may use at most 64 MiB of HBM per device.

v0:
```python
import jax
import jax.numpy as jnp
from jax import lax
from jax.sharding import PartitionSpec as P

HEADS = 8
HEAD = 128
CH = 1024
KSIZE = 31
BLOCK = 64


EPS = 1e-06
HIGH = lax.Precision.HIGHEST


def in_order(pieces, dim):
    shape = list(pieces.shape[1:])
    shape[dim] *= pieces.shape[0]
    return jnp.moveaxis(pieces, 0, dim).reshape(shape)


def sent_to_all(x, axis):
    size = lax.axis_size(axis)
    return lax.all_to_all(jnp.broadcast_to(x[None], (size, *x.shape)), axis, 0, 0, tiled=True)


def gathered_copies(x, axis, dim):
    return in_order(sent_to_all(x, axis), dim)


def in_one_piece(arrays, axis, dim, along):
    both = jnp.concatenate(arrays, axis=along)
    result, at, gathered = (lax.all_gather(both, axis, axis=dim, tiled=True), 0, [])
    for a in arrays:
        gathered.append(lax.slice_in_dim(result, at, at + a.shape[along], axis=along))
        at += a.shape[along]
    return tuple(gathered)


def from_behind(block, axis, distance):
    devices = range(lax.axis_size(axis))
    route = [(i - distance, i) for i in devices if i - distance in devices]
    return lax.ppermute(block, axis, route)


def over_pieces(x, axis):
    return lax.all_gather(x, axis).sum(0)


def cut_along(x, dim, size):
    shape = x.shape
    pieces = x.reshape(*shape[:dim], size, shape[dim] // size, *shape[dim + 1 :])
    return jnp.moveaxis(pieces, dim, 0)


def summed_on_arrival(x, axis, dim):
    size = lax.axis_size(axis)
    pieces = lax.all_to_all(cut_along(x, dim, size), axis, 0, 0, tiled=True)
    return jnp.sum(pieces.astype(jnp.float32), axis=0)


def unit_rows(values):
    return values * lax.rsqrt(jnp.sum(values * values, axis=-1, keepdims=True) + EPS)


def rounded(values):
    return lax.optimization_barrier(values.astype(jnp.bfloat16)).astype(jnp.float32)


def block_terms(query, keys, values, log_decay, beta, blen):
    rows = keys.shape[0]
    count = rows // blen

    def split_blocks(array):
        return jnp.swapaxes(array.reshape((count, blen) + array.shape[1:]), 1, 2)

    q_blocks, k_blocks, v_blocks = (split_blocks(query), split_blocks(keys), split_blocks(values))
    g_blocks, b_blocks = (split_blocks(log_decay), split_blocks(beta))
    cumdec = jnp.cumsum(g_blocks, axis=-1)
    lower = jnp.tril(jnp.ones((blen, blen), bool))
    strict = jnp.tril(jnp.ones((blen, blen), bool), -1)
    diff = cumdec[..., :, None] - cumdec[..., None, :]
    gamma = jnp.where(lower, jnp.exp(jnp.where(lower, diff, 0.0)), 0.0)
    k_beta = k_blocks * b_blocks[..., None]
    a_matrix = jnp.where(
        strict, jnp.einsum("nhid,nhjd->nhij", k_beta, k_blocks, precision=HIGH) * gamma, 0.0
    )
    left_side = a_matrix + jnp.eye(blen, dtype=jnp.float32)
    right_side = jnp.concatenate(
        [v_blocks * b_blocks[..., None], k_beta * jnp.exp(cumdec)[..., None]], axis=-1
    )
    solved = jax.scipy.linalg.solve_triangular(
        left_side, right_side, lower=True, unit_diagonal=True
    )
    width_v = v_blocks.shape[-1]
    updates, w_rows = (solved[..., :width_v], solved[..., width_v:])
    q_k = jnp.where(
        lower, jnp.einsum("nhid,nhjd->nhij", q_blocks, k_blocks, precision=HIGH) * gamma, 0.0
    )
    last = cumdec[..., -1]
    k_decayed = k_blocks * jnp.exp(last[..., None] - cumdec)[..., None]
    q_decayed = q_blocks * jnp.exp(cumdec)[..., None]
    return (q_decayed, k_decayed, updates, w_rows, q_k, last)


def device_map(terms, width_k, width_v, heads):
    q_decayed, k_decayed, updates, w_rows, q_k, last = terms
    identity = jnp.broadcast_to(jnp.eye(width_k, dtype=jnp.float32), (heads, width_k, width_k))

    def compose(carry, input_rows):
        maps, offsets = carry
        k_part, u_part, w_part, last_part = input_rows
        step_map = jnp.exp(last_part)[:, None, None] * identity - jnp.einsum(
            "hcd,hce->hde", k_part, w_part, precision=HIGH
        )
        maps = jnp.einsum("hde,hef->hdf", step_map, maps, precision=HIGH)
        offsets = jnp.einsum("hde,hef->hdf", step_map, offsets, precision=HIGH) + jnp.einsum(
            "hcd,hce->hde", k_part, u_part, precision=HIGH
        )
        return ((maps, offsets), None)

    start = (identity, jnp.zeros((heads, width_k, width_v), jnp.float32))
    (maps, offsets), _ = lax.scan(compose, start, (k_decayed, updates, w_rows, last))
    return (maps, offsets, identity)


def block_outputs(start_state, terms):

    def advance(state, input_rows):
        q_decayed, k_decayed, updates, w_rows, q_k, last = input_rows
        v_new = updates - jnp.einsum("hcd,hde->hce", w_rows, state, precision=HIGH)
        output = jnp.einsum("hcd,hde->hce", q_decayed, state, precision=HIGH) + jnp.einsum(
            "hij,hje->hie", q_k, v_new, precision=HIGH
        )
        state = state * jnp.exp(last)[..., None, None] + jnp.einsum(
            "hcd,hce->hde", k_decayed, v_new, precision=HIGH
        )
        return (state, output)

    _, outputs = lax.scan(advance, start_state, terms)
    count, heads, blen, width_v = outputs.shape
    return jnp.swapaxes(outputs, 1, 2).reshape(count * blen, heads, width_v)


def apply_map(maps, state):
    return jnp.einsum("hde,hef->hdf", maps, state, precision=HIGH)


def on_device(
    tokens,
    input_norm_gain,
    query_weight,
    key_weight,
    value_weight,
    decay_gate_weight,
    write_strength_weight,
    up_weight,
    gate_half_weight,
    log_decay_rate,
    write_strength_bias,
    decay_spike_added,
    starting_state,
    head_norm_gain,
    convolution_kernel,
    channel_norm_gain,
    delta_output_rows,
    convolution_output_rows,
):
    rows = tokens.shape[1]
    heads_here = query_weight.shape[1] // HEAD
    chan_here = up_weight.shape[1]
    tp_index = lax.axis_index("tp")
    sp_index = lax.axis_index("sp")
    gathered = gathered_copies(tokens[0], "tp", 1)
    token_f = gathered.astype(jnp.float32)
    normed = (
        token_f
        * lax.rsqrt(jnp.mean(token_f * token_f, axis=-1, keepdims=True) + EPS)
        * input_norm_gain
    ).astype(jnp.bfloat16)
    pieces = in_one_piece(
        (query_weight, key_weight, value_weight, up_weight, gate_half_weight), "sp", 0, 1
    )
    q_sum, k_sum, v_sum, up_sum, gate_sum = tuple(
        (jnp.dot(normed, piece, preferred_element_type=jnp.float32) for piece in pieces)
    )
    glu = lax.optimization_barrier(
        (rounded(up_sum) * jax.nn.sigmoid(rounded(gate_sum))).astype(jnp.bfloat16)
    )
    rim = from_behind(glu[rows - (KSIZE - 1) :], "sp", 1)
    shape = (rows, heads_here, HEAD)
    query = unit_rows(jax.nn.silu(rounded(q_sum)).reshape(shape)) * HEAD ** (-0.5)
    keys = unit_rows(jax.nn.silu(rounded(k_sum)).reshape(shape))
    values = jax.nn.silu(rounded(v_sum)).reshape(shape)
    gate_cols = jnp.concatenate([decay_gate_weight, write_strength_weight], axis=1)
    small_raw = rounded(jnp.dot(normed, gate_cols, preferred_element_type=jnp.float32))
    head_start = tp_index * heads_here
    decay_logits = lax.dynamic_slice_in_dim(small_raw[:, :HEADS], head_start, heads_here, 1)
    beta_raw = lax.dynamic_slice_in_dim(small_raw[:, HEADS:], head_start, heads_here, 1)
    decay_rates = jnp.exp(lax.dynamic_slice_in_dim(log_decay_rate, head_start, heads_here, 0))
    bias_here = lax.dynamic_slice_in_dim(write_strength_bias, head_start, heads_here, 0)
    log_decay = -decay_rates * jax.nn.softplus(decay_logits) + decay_spike_added[0]
    beta = jax.nn.sigmoid(beta_raw + bias_here)
    terms = block_terms(query, keys, values, log_decay, beta, BLOCK)
    maps, offsets, identity = device_map(terms, HEAD, HEAD, heads_here)
    start_state = starting_state[0]
    first = sp_index == 0

    def relay(turn, incoming):
        outgoing = apply_map(maps, incoming) + offsets
        arrived = from_behind(outgoing.astype(jnp.bfloat16), "sp", 1).astype(outgoing.dtype)
        return jnp.where(first, start_state, arrived)

    state_in = lax.fori_loop(
        0,
        lax.axis_size("sp") - 1,
        relay,
        jnp.where(first, start_state, jnp.zeros_like(start_state)),
    )
    extended = jnp.concatenate([rim, glu], axis=0).astype(jnp.float32)
    taps_here = lax.dynamic_slice_in_dim(convolution_kernel, tp_index * chan_here, chan_here, 1)
    conv = jnp.zeros((rows, chan_here), jnp.float32)
    for tap in range(KSIZE):
        conv = conv + taps_here[tap] * extended[tap : tap + rows]
    row_sum, row_squares = (
        over_pieces(jnp.sum(conv, axis=-1), "tp"),
        over_pieces(jnp.sum(conv * conv, axis=-1), "tp"),
    )
    mean_c = (row_sum / CH)[:, None]
    var_c = (row_squares / CH)[:, None] - mean_c * mean_c
    gain_here = lax.dynamic_slice_in_dim(channel_norm_gain, tp_index * chan_here, chan_here, 0)
    conv_out = jax.nn.silu((conv - mean_c) * lax.rsqrt(var_c + EPS) * gain_here).astype(
        jnp.bfloat16
    )
    attn = block_outputs(state_in, terms)
    attn_out = (
        attn * lax.rsqrt(jnp.mean(attn * attn, axis=-1, keepdims=True) + EPS) * head_norm_gain
    ).astype(jnp.bfloat16)
    attn_out = attn_out.reshape(rows, heads_here * HEAD)
    pieces = in_one_piece((delta_output_rows, convolution_output_rows), "sp", 1, 0)
    term = jnp.dot(attn_out, pieces[0], preferred_element_type=jnp.float32) + jnp.dot(
        conv_out, pieces[1], preferred_element_type=jnp.float32
    )
    mixed = summed_on_arrival(term.astype(jnp.bfloat16), "tp", 1).astype(jnp.bfloat16)
    return mixed[None]


def solution(mesh):
    return jax.shard_map(
        on_device,
        mesh=mesh,
        in_specs=(
            P(("grp", "fs"), "sp", "tp"),
            P(),
            P("sp", "tp"),
            P("sp", "tp"),
            P("sp", "tp"),
            P(),
            P(),
            P("sp", "tp"),
            P("sp", "tp"),
            P(),
            P(),
            P(("grp", "fs"), "sp", "tp"),
            P(("grp", "fs"), "tp", None, None),
            P(),
            P(),
            P(),
            P("tp", "sp"),
            P("tp", "sp"),
        ),
        out_specs=P(("grp", "fs"), "sp", "tp"),
        check_vma=False,
    )
```

profile of v0, /device:TPU:33, one launch (start us, length us, event | category | flops | bytes accessed | tf_op | source)
XLA Modules:
  0.0 439.2 jit_solution(8331409701187650415)
XLA Ops:
  13.4 24.1 %all-to-all-start = ((bf16[2,256,1024]{1,2,0:T(8,128)(2,1)}), bf16[2,256,1024]{1,2,0:T(8,128)(2,1)S(1)}, u32[]{:S(2)}, u32[]{:S(2)}) async-start(bf16[2,256,1024]{1,2,0:T(8,128)(2,1)} %broadcast_in_dim.67), calls=%async_computation | async-start | bytes 2097152 | tf_op jit(solution)/shard_map/all_to_all | solution.py:25
  45.8 2.1 constant_dynamic-slice_fusion.2
  47.8 104.0 %all-gather.7.cloned.1.call-done = bf16[2048,2560]{1,0:T(8,128)(2,1)} async-done(((bf16[128,2560]{1,0:T(8,128)(2,1)}), bf16[2048,2560]{1,0:T(8,128)(2,1)}) %all-gather.7.cloned.1.call-update) | async-done | bytes 10485776 | tf_op jit(solution)/shard_map/all_gather | solution.py:34
  151.9 2.3 fusion.68
  154.2 2.3 fusion.71
  158.0 2.3 fusion.59
  163.2 2.3 fusion.65
  170.2 2.5 fusion.62
  175.2 79.5 %custom-call.4 = f32[4,4,1,64,64]{3,4,2,1,0:T(8,128)} custom-call(f32[4,4,1,64,64]{4,3,2,1,0:T(8,128)S(1)} %fusion.58), custom_call_target="InvertDiagBlocksLowerTriangular" | custom-call | tf_op jit(solution)/shard_map/jit(_solve_triangular)/vmap(vmap())/triangular_solve | solution.py:93
  254.7 2.0 fusion.53
  256.7 1.9 multiply_multiply_fusion
  259.9 11.0 %while.37 = (s32[]{:T(128)}, f32[4,128,128]{2,1,0:T(8,128)S(1)}, f32[4,128,128]{2,1,0:T(8,128)S(1)}, f32[4,4]{1,0:T(4,128)}, f32[4,4,64,128]{3,2,1,0:T(8,128)S(1...) while((s32[]{:T(128)}, f32[4,128,128]{2,1,0:T(8,128)S(1)}, ...), condition=%wide.region_4.5_spmd.clone, body=%wide.region_3.4_spmd.clone.sunk | while | flops 302252032 | bytes 3476115 | solution.py:124
  270.9 107.7 %while.35 = (s32[]{:T(128)}, f32[4,128,128]{2,1,0:T(8,128)S(1)}, pred[]{:T(512)}, f32[4,128,128]{2,1,0:T(8,128)S(1)}, f32[4,128,128]{2,1,0:T(8,128)S(1)}, /*index=5*/f32[4,128,128]{2,1,0:T(8,128)S(1)}, s32[]{:T(128)}) while((s32[]{:T(128)}, f32[4,128,128]{2,1,0:T(8,128)S(1)}, pred[]{:T(512)}, f32[4,128,128]{2,1,0:T(8,128)S(1)}, ...), condition=%wide.region_6.7_spmd, body=%wide.region_5.6_spmd.sunk | while | flops 100925440 | bytes 2097270 | solution.py:215
  271.3 3.0 collective-permute-start
  274.3 1.9 collective-permute-done
  276.7 4.3 collective-permute-start
  281.0 1.9 collective-permute-done
  283.4 3.8 collective-permute-start
  287.2 1.9 collective-permute-done
  289.6 3.8 collective-permute-start
  293.4 1.9 collective-permute-done
  295.8 3.8 collective-permute-start
  299.6 1.9 collective-permute-done
  302.0 5.0 %collective-permute-start = (bf16[4,128,128]{2,1,0:T(8,128)(2,1)S(1)}, bf16[4,128,128]{2,1,0:T(8,128)(2,1)S(1)}, u32[]{:S(2)}, u32[]{:S(2)}) collective-permute-start(bf16[4,128,128]{2,1,0:T(8,128)(2,1)S(1)} %fusion.200), channel_id=1, source_target_pairs={{0,8},{8,16},{16,24},{24,32},{32,40},{40,48},{48,56},{56,64},{64,7... | collective-permute-start | bytes 393224 | tf_op jit(solution)/shard_map/while/body/eval_jaxpr/ppermute | solution.py:44
  307.0 1.9 collective-permute-done
  309.3 5.0 %collective-permute-start = (bf16[4,128,128]{2,1,0:T(8,128)(2,1)S(1)}, bf16[4,128,128]{2,1,0:T(8,128)(2,1)S(1)}, u32[]{:S(2)}, u32[]{:S(2)}) collective-permute-start(bf16[4,128,128]{2,1,0:T(8,128)(2,1)S(1)} %fusion.200), channel_id=1, source_target_pairs={{0,8},{8,16},{16,24},{24,32},{32,40},{40,48},{48,56},{56,64},{64,7... | collective-permute-start | bytes 393224 | tf_op jit(solution)/shard_map/while/body/eval_jaxpr/ppermute | solution.py:44
  314.4 2.3 collective-permute-done
  317.1 5.3 %collective-permute-start = (bf16[4,128,128]{2,1,0:T(8,128)(2,1)S(1)}, bf16[4,128,128]{2,1,0:T(8,128)(2,1)S(1)}, u32[]{:S(2)}, u32[]{:S(2)}) collective-permute-start(bf16[4,128,128]{2,1,0:T(8,128)(2,1)S(1)} %fusion.200), channel_id=1, source_target_pairs={{0,8},{8,16},{16,24},{24,32},{32,40},{40,48},{48,56},{56,64},{64,7... | collective-permute-start | bytes 393224 | tf_op jit(solution)/shard_map/while/body/eval_jaxpr/ppermute | solution.py:44
  322.5 3.1 collective-permute-done
  326.0 5.2 %collective-permute-start = (bf16[4,128,128]{2,1,0:T(8,128)(2,1)S(1)}, bf16[4,128,128]{2,1,0:T(8,128)(2,1)S(1)}, u32[]{:S(2)}, u32[]{:S(2)}) collective-permute-start(bf16[4,128,128]{2,1,0:T(8,128)(2,1)S(1)} %fusion.200), channel_id=1, source_target_pairs={{0,8},{8,16},{16,24},{24,32},{32,40},{40,48},{48,56},{56,64},{64,7... | collective-permute-start | bytes 393224 | tf_op jit(solution)/shard_map/while/body/eval_jaxpr/ppermute | solution.py:44
  331.2 1.9 collective-permute-done
  333.6 5.2 %collective-permute-start = (bf16[4,128,128]{2,1,0:T(8,128)(2,1)S(1)}, bf16[4,128,128]{2,1,0:T(8,128)(2,1)S(1)}, u32[]{:S(2)}, u32[]{:S(2)}) collective-permute-start(bf16[4,128,128]{2,1,0:T(8,128)(2,1)S(1)} %fusion.200), channel_id=1, source_target_pairs={{0,8},{8,16},{16,24},{24,32},{32,40},{40,48},{48,56},{56,64},{64,7... | collective-permute-start | bytes 393224 | tf_op jit(solution)/shard_map/while/body/eval_jaxpr/ppermute | solution.py:44
  338.8 1.9 collective-permute-done
  341.2 5.0 %collective-permute-start = (bf16[4,128,128]{2,1,0:T(8,128)(2,1)S(1)}, bf16[4,128,128]{2,1,0:T(8,128)(2,1)S(1)}, u32[]{:S(2)}, u32[]{:S(2)}) collective-permute-start(bf16[4,128,128]{2,1,0:T(8,128)(2,1)S(1)} %fusion.200), channel_id=1, source_target_pairs={{0,8},{8,16},{16,24},{24,32},{32,40},{40,48},{48,56},{56,64},{64,7... | collective-permute-start | bytes 393224 | tf_op jit(solution)/shard_map/while/body/eval_jaxpr/ppermute | solution.py:44
  346.2 1.9 collective-permute-done
  348.6 5.4 %collective-permute-start = (bf16[4,128,128]{2,1,0:T(8,128)(2,1)S(1)}, bf16[4,128,128]{2,1,0:T(8,128)(2,1)S(1)}, u32[]{:S(2)}, u32[]{:S(2)}) collective-permute-start(bf16[4,128,128]{2,1,0:T(8,128)(2,1)S(1)} %fusion.200), channel_id=1, source_target_pairs={{0,8},{8,16},{16,24},{24,32},{32,40},{40,48},{48,56},{56,64},{64,7... | collective-permute-start | bytes 393224 | tf_op jit(solution)/shard_map/while/body/eval_jaxpr/ppermute | solution.py:44
  353.9 1.9 collective-permute-done
  356.3 5.0 %collective-permute-start = (bf16[4,128,128]{2,1,0:T(8,128)(2,1)S(1)}, bf16[4,128,128]{2,1,0:T(8,128)(2,1)S(1)}, u32[]{:S(2)}, u32[]{:S(2)}) collective-permute-start(bf16[4,128,128]{2,1,0:T(8,128)(2,1)S(1)} %fusion.200), channel_id=1, source_target_pairs={{0,8},{8,16},{16,24},{24,32},{32,40},{40,48},{48,56},{56,64},{64,7... | collective-permute-start | bytes 393224 | tf_op jit(solution)/shard_map/while/body/eval_jaxpr/ppermute | solution.py:44
  363.7 5.0 %collective-permute-start = (bf16[4,128,128]{2,1,0:T(8,128)(2,1)S(1)}, bf16[4,128,128]{2,1,0:T(8,128)(2,1)S(1)}, u32[]{:S(2)}, u32[]{:S(2)}) collective-permute-start(bf16[4,128,128]{2,1,0:T(8,128)(2,1)S(1)} %fusion.200), channel_id=1, source_target_pairs={{0,8},{8,16},{16,24},{24,32},{32,40},{40,48},{48,56},{56,64},{64,7... | collective-permute-start | bytes 393224 | tf_op jit(solution)/shard_map/while/body/eval_jaxpr/ppermute | solution.py:44
  368.7 1.9 collective-permute-done
  371.1 5.0 %collective-permute-start = (bf16[4,128,128]{2,1,0:T(8,128)(2,1)S(1)}, bf16[4,128,128]{2,1,0:T(8,128)(2,1)S(1)}, u32[]{:S(2)}, u32[]{:S(2)}) collective-permute-start(bf16[4,128,128]{2,1,0:T(8,128)(2,1)S(1)} %fusion.200), channel_id=1, source_target_pairs={{0,8},{8,16},{16,24},{24,32},{32,40},{40,48},{48,56},{56,64},{64,7... | collective-permute-start | bytes 393224 | tf_op jit(solution)/shard_map/while/body/eval_jaxpr/ppermute | solution.py:44
  376.1 2.5 collective-permute-done
  378.6 15.7 %while.36 = (s32[]{:T(128)}, f32[4,128,128]{2,1,0:T(8,128)S(1)}, f32[4,4,64,128]{3,2,1,0:T(8,128)}, f32[4,4]{1,0:T(4,128)}, f32[4,4,64,128]{3,2,1,0:T(8,128)S(1)...) while((s32[]{:T(128)}, f32[4,128,128]{2,1,0:T(8,128)S(1)}, ...), condition=%wide.region_9.10_spmd, body=%wide.region_8.9_spmd.sunk | while | flops 176357376 | bytes 2493581 | solution.py:141
  397.8 2.3 fusion.43
  400.5 2.7 fusion.151
  403.2 19.0 %all-gather.2 = f32[2,1,256]{2,1,0:T(1,128)S(1)} all-gather(f32[1,1,256]{2,1,0:T(1,128)S(1)} %bitcast.238), channel_id=2, replica_groups=mesh['grp'=2,'sp'=16,'fs'=4,'tp'=2] {'tp'}, dimensions={0}, use_global_device_ids=true | all-gather | bytes 3072 | tf_op jit(solution)/shard_map/all_gather | solution.py:48
  424.1 2.5 fusion.37
  426.7 4.6 %all_to_all.10 = bf16[2,256,1024]{2,1,0:T(8,128)(2,1)S(1)} all-to-all(bf16[2,256,1024]{2,1,0:T(8,128)(2,1)S(1)} %bitcast.195), channel_id=1, replica_groups=mesh['grp'=2,'sp'=16,'fs'=4,'tp'=2] {'tp'}, dimensions={0} | all-to-all | bytes 2097152 | tf_op jit(solution)/shard_map/all_to_all | solution.py:59
  (242 shorter events, 68.6 us)
Async XLA Ops:
  6.5 36.7 %copy-start = (f32[128]{0:T(128)S(1)}, f32[128]{0:T(128)}, u32[]{:S(2)}) copy-start(f32[128]{0:T(128)} %param.37) | copy-start | bytes 1540
  6.6 5.6 %copy-start.7 = (bf16[1,256,1024]{2,1,0:T(8,128)(2,1)S(1)}, bf16[1,256,1024]{2,1,0:T(8,128)(2,1)}, u32[]{:S(2)}) copy-start(bf16[1,256,1024]{2,1,0:T(8,128)(2,1)} %param.24) | copy-start | bytes 1572868
  6.6 145.3 %all-gather.7.cloned.1.call-start = ((), (), s32[]{:S(2)}) async-start(), calls=%async_computation.2 | async-start | bytes 11141120 | tf_op jit(solution)/shard_map/all_gather | solution.py:34
  12.1 25.4 %copy-start.8 = (bf16[512,128]{1,0:T(8,128)(2,1)S(1)}, bf16[512,128]{1,0:T(8,128)(2,1)}, u32[]{:S(2)}) copy-start(bf16[512,128]{1,0:T(8,128)(2,1)} %param.41) | copy-start | bytes 393220
  12.2 25.4 %copy-start.9 = (bf16[512,128]{1,0:T(8,128)(2,1)S(1)}, bf16[512,128]{1,0:T(8,128)(2,1)}, u32[]{:S(2)}) copy-start(bf16[512,128]{1,0:T(8,128)(2,1)} %param.40) | copy-start | bytes 393220
  13.4 26.2 %copy-start.45 = (f32[8]{0:T(128)S(1)}, f32[8]{0:T(128)}, u32[]{:S(2)}) copy-start(f32[8]{0:T(128)} %param.34) | copy-start | bytes 100
  13.4 26.3 %copy-start.46 = (f32[8]{0:T(128)S(1)}, f32[8]{0:T(128)}, u32[]{:S(2)}) copy-start(f32[8]{0:T(128)} %param.33) | copy-start | bytes 100
  13.4 26.4 %copy-start.12 = (f32[2048]{0:T(1024)S(1)}, f32[2048]{0:T(1024)}, u32[]{:S(2)}) copy-start(f32[2048]{0:T(1024)} %param.25) | copy-start | bytes 24580
  13.4 25.9 %all-to-all-start = ((bf16[2,256,1024]{1,2,0:T(8,128)(2,1)}), bf16[2,256,1024]{1,2,0:T(8,128)(2,1)S(1)}, u32[]{:S(2)}, u32[]{:S(2)}) async-start(bf16[2,256,1024]{1,2,0:T(8,128)(2,1)} %broadcast_in_dim.67), calls=%async_computation | async-start | bytes 2097152 | tf_op jit(solution)/shard_map/all_to_all | solution.py:25
  37.6 359.6 %all-gather.9.cloned.1.call-start = ((), (), s32[]{:S(2)}) async-start(), calls=%async_computation.3 | async-start | bytes 4456448 | tf_op jit(solution)/shard_map/all_gather | solution.py:34
  38.4 4.8 %copy-start.1 = (f32[1,4,128,128]{3,2,1,0:T(8,128)S(1)}, f32[1,4,128,128]{3,2,1,0:T(8,128)}, u32[]{:S(2)}) copy-start(f32[1,4,128,128]{3,2,1,0:T(8,128)} %param.36) | copy-start | bytes 786436
  39.6 3.7 copy-start.44
  156.7 243.4 %collective-permute-start.1 = (bf16[30,512]{1,0:T(8,128)(2,1)S(1)}, bf16[30,512]{1,0:T(8,128)(2,1)S(1)}, u32[]{:S(2)}, u32[]{:S(2)}) collective-permute-start(bf16[30,512]{1,0:T(8,128)(2,1)S(1)} %slice.317), channel_id=1, source_target_pairs={{0,8},{8,16},{16,24},{24,32},{32,40},{40,48},{48,56},{56,64},{64,7... | collective-permute-start | bytes 92168 | tf_op jit(solution)/shard_map/ppermute | solution.py:44
  170.2 84.5 %copy-start.2 = (f32[4,64,4,128]{3,2,1,0:T(4,128)}, f32[4,64,4,128]{3,2,1,0:T(4,128)S(1)}, u32[]{:S(2)}) copy-start(f32[4,64,4,128]{3,2,1,0:T(4,128)S(1)} %reshape.142) | copy-start | bytes 1572868
  271.3 4.9 %collective-permute-start = (bf16[4,128,128]{2,1,0:T(8,128)(2,1)S(1)}, bf16[4,128,128]{2,1,0:T(8,128)(2,1)S(1)}, u32[]{:S(2)}, u32[]{:S(2)}) collective-permute-start(bf16[4,128,128]{2,1,0:T(8,128)(2,1)S(1)} %fusion.200), channel_id=1, source_target_pairs={{0,8},{8,16},{16,24},{24,32},{32,40},{40,48},{48,56},{56,64},{64,7... | collective-permute-start | bytes 393224 | tf_op jit(solution)/shard_map/while/body/eval_jaxpr/ppermute | solution.py:44
  276.7 6.2 %collective-permute-start = (bf16[4,128,128]{2,1,0:T(8,128)(2,1)S(1)}, bf16[4,128,128]{2,1,0:T(8,128)(2,1)S(1)}, u32[]{:S(2)}, u32[]{:S(2)}) collective-permute-start(bf16[4,128,128]{2,1,0:T(8,128)(2,1)S(1)} %fusion.200), channel_id=1, source_target_pairs={{0,8},{8,16},{16,24},{24,32},{32,40},{40,48},{48,56},{56,64},{64,7... | collective-permute-start | bytes 393224 | tf_op jit(solution)/shard_map/while/body/eval_jaxpr/ppermute | solution.py:44
  283.4 5.7 %collective-permute-start = (bf16[4,128,128]{2,1,0:T(8,128)(2,1)S(1)}, bf16[4,128,128]{2,1,0:T(8,128)(2,1)S(1)}, u32[]{:S(2)}, u32[]{:S(2)}) collective-permute-start(bf16[4,128,128]{2,1,0:T(8,128)(2,1)S(1)} %fusion.200), channel_id=1, source_target_pairs={{0,8},{8,16},{16,24},{24,32},{32,40},{40,48},{48,56},{56,64},{64,7... | collective-permute-start | bytes 393224 | tf_op jit(solution)/shard_map/while/body/eval_jaxpr/ppermute | solution.py:44
  289.6 5.7 %collective-permute-start = (bf16[4,128,128]{2,1,0:T(8,128)(2,1)S(1)}, bf16[4,128,128]{2,1,0:T(8,128)(2,1)S(1)}, u32[]{:S(2)}, u32[]{:S(2)}) collective-permute-start(bf16[4,128,128]{2,1,0:T(8,128)(2,1)S(1)} %fusion.200), channel_id=1, source_target_pairs={{0,8},{8,16},{16,24},{24,32},{32,40},{40,48},{48,56},{56,64},{64,7... | collective-permute-start | bytes 393224 | tf_op jit(solution)/shard_map/while/body/eval_jaxpr/ppermute | solution.py:44
  295.8 5.7 %collective-permute-start = (bf16[4,128,128]{2,1,0:T(8,128)(2,1)S(1)}, bf16[4,128,128]{2,1,0:T(8,128)(2,1)S(1)}, u32[]{:S(2)}, u32[]{:S(2)}) collective-permute-start(bf16[4,128,128]{2,1,0:T(8,128)(2,1)S(1)} %fusion.200), channel_id=1, source_target_pairs={{0,8},{8,16},{16,24},{24,32},{32,40},{40,48},{48,56},{56,64},{64,7... | collective-permute-start | bytes 393224 | tf_op jit(solution)/shard_map/while/body/eval_jaxpr/ppermute | solution.py:44
  302.0 6.9 %collective-permute-start = (bf16[4,128,128]{2,1,0:T(8,128)(2,1)S(1)}, bf16[4,128,128]{2,1,0:T(8,128)(2,1)S(1)}, u32[]{:S(2)}, u32[]{:S(2)}) collective-permute-start(bf16[4,128,128]{2,1,0:T(8,128)(2,1)S(1)} %fusion.200), channel_id=1, source_target_pairs={{0,8},{8,16},{16,24},{24,32},{32,40},{40,48},{48,56},{56,64},{64,7... | collective-permute-start | bytes 393224 | tf_op jit(solution)/shard_map/while/body/eval_jaxpr/ppermute | solution.py:44
  309.3 7.3 %collective-permute-start = (bf16[4,128,128]{2,1,0:T(8,128)(2,1)S(1)}, bf16[4,128,128]{2,1,0:T(8,128)(2,1)S(1)}, u32[]{:S(2)}, u32[]{:S(2)}) collective-permute-start(bf16[4,128,128]{2,1,0:T(8,128)(2,1)S(1)} %fusion.200), channel_id=1, source_target_pairs={{0,8},{8,16},{16,24},{24,32},{32,40},{40,48},{48,56},{56,64},{64,7... | collective-permute-start | bytes 393224 | tf_op jit(solution)/shard_map/while/body/eval_jaxpr/ppermute | solution.py:44
  317.1 8.4 %collective-permute-start = (bf16[4,128,128]{2,1,0:T(8,128)(2,1)S(1)}, bf16[4,128,128]{2,1,0:T(8,128)(2,1)S(1)}, u32[]{:S(2)}, u32[]{:S(2)}) collective-permute-start(bf16[4,128,128]{2,1,0:T(8,128)(2,1)S(1)} %fusion.200), channel_id=1, source_target_pairs={{0,8},{8,16},{16,24},{24,32},{32,40},{40,48},{48,56},{56,64},{64,7... | collective-permute-start | bytes 393224 | tf_op jit(solution)/shard_map/while/body/eval_jaxpr/ppermute | solution.py:44
  326.0 7.1 %collective-permute-start = (bf16[4,128,128]{2,1,0:T(8,128)(2,1)S(1)}, bf16[4,128,128]{2,1,0:T(8,128)(2,1)S(1)}, u32[]{:S(2)}, u32[]{:S(2)}) collective-permute-start(bf16[4,128,128]{2,1,0:T(8,128)(2,1)S(1)} %fusion.200), channel_id=1, source_target_pairs={{0,8},{8,16},{16,24},{24,32},{32,40},{40,48},{48,56},{56,64},{64,7... | collective-permute-start | bytes 393224 | tf_op jit(solution)/shard_map/while/body/eval_jaxpr/ppermute | solution.py:44
  333.6 7.2 %collective-permute-start = (bf16[4,128,128]{2,1,0:T(8,128)(2,1)S(1)}, bf16[4,128,128]{2,1,0:T(8,128)(2,1)S(1)}, u32[]{:S(2)}, u32[]{:S(2)}) collective-permute-start(bf16[4,128,128]{2,1,0:T(8,128)(2,1)S(1)} %fusion.200), channel_id=1, source_target_pairs={{0,8},{8,16},{16,24},{24,32},{32,40},{40,48},{48,56},{56,64},{64,7... | collective-permute-start | bytes 393224 | tf_op jit(solution)/shard_map/while/body/eval_jaxpr/ppermute | solution.py:44
  341.2 6.9 %collective-permute-start = (bf16[4,128,128]{2,1,0:T(8,128)(2,1)S(1)}, bf16[4,128,128]{2,1,0:T(8,128)(2,1)S(1)}, u32[]{:S(2)}, u32[]{:S(2)}) collective-permute-start(bf16[4,128,128]{2,1,0:T(8,128)(2,1)S(1)} %fusion.200), channel_id=1, source_target_pairs={{0,8},{8,16},{16,24},{24,32},{32,40},{40,48},{48,56},{56,64},{64,7... | collective-permute-start | bytes 393224 | tf_op jit(solution)/shard_map/while/body/eval_jaxpr/ppermute | solution.py:44
  348.6 7.3 %collective-permute-start = (bf16[4,128,128]{2,1,0:T(8,128)(2,1)S(1)}, bf16[4,128,128]{2,1,0:T(8,128)(2,1)S(1)}, u32[]{:S(2)}, u32[]{:S(2)}) collective-permute-start(bf16[4,128,128]{2,1,0:T(8,128)(2,1)S(1)} %fusion.200), channel_id=1, source_target_pairs={{0,8},{8,16},{16,24},{24,32},{32,40},{40,48},{48,56},{56,64},{64,7... | collective-permute-start | bytes 393224 | tf_op jit(solution)/shard_map/while/body/eval_jaxpr/ppermute | solution.py:44
  356.3 7.0 %collective-permute-start = (bf16[4,128,128]{2,1,0:T(8,128)(2,1)S(1)}, bf16[4,128,128]{2,1,0:T(8,128)(2,1)S(1)}, u32[]{:S(2)}, u32[]{:S(2)}) collective-permute-start(bf16[4,128,128]{2,1,0:T(8,128)(2,1)S(1)} %fusion.200), channel_id=1, source_target_pairs={{0,8},{8,16},{16,24},{24,32},{32,40},{40,48},{48,56},{56,64},{64,7... | collective-permute-start | bytes 393224 | tf_op jit(solution)/shard_map/while/body/eval_jaxpr/ppermute | solution.py:44
  363.7 7.0 %collective-permute-start = (bf16[4,128,128]{2,1,0:T(8,128)(2,1)S(1)}, bf16[4,128,128]{2,1,0:T(8,128)(2,1)S(1)}, u32[]{:S(2)}, u32[]{:S(2)}) collective-permute-start(bf16[4,128,128]{2,1,0:T(8,128)(2,1)S(1)} %fusion.200), channel_id=1, source_target_pairs={{0,8},{8,16},{16,24},{24,32},{32,40},{40,48},{48,56},{56,64},{64,7... | collective-permute-start | bytes 393224 | tf_op jit(solution)/shard_map/while/body/eval_jaxpr/ppermute | solution.py:44
  371.1 7.5 %collective-permute-start = (bf16[4,128,128]{2,1,0:T(8,128)(2,1)S(1)}, bf16[4,128,128]{2,1,0:T(8,128)(2,1)S(1)}, u32[]{:S(2)}, u32[]{:S(2)}) collective-permute-start(bf16[4,128,128]{2,1,0:T(8,128)(2,1)S(1)} %fusion.200), channel_id=1, source_target_pairs={{0,8},{8,16},{16,24},{24,32},{32,40},{40,48},{48,56},{56,64},{64,7... | collective-permute-start | bytes 393224 | tf_op jit(solution)/shard_map/while/body/eval_jaxpr/ppermute | solution.py:44
  397.5 2.7 copy-start.13
  397.5 2.7 copy-start.14
  397.5 2.7 copy-start.15
  397.5 2.7 copy-start.16
  397.5 2.7 copy-start.17
  397.5 2.7 copy-start.18
  397.5 2.7 copy-start.19
  397.5 2.7 copy-start.20
  397.6 2.7 copy-start.21
  397.6 2.7 copy-start.22
  397.6 2.7 copy-start.23
  397.6 2.7 copy-start.24
  397.6 2.7 copy-start.25
  397.6 2.7 copy-start.26
  397.6 2.7 copy-start.27
  397.6 2.7 copy-start.28
  397.6 2.7 copy-start.29
  397.6 2.7 copy-start.30
  400.5 23.6 %copy-start.43 = (f32[512]{0:T(512)S(1)}, f32[512]{0:T(512)}, u32[]{:S(2)}) copy-start(f32[512]{0:T(512)} %dynamic_slice.56) | copy-start | bytes 6148
  (18 other events, 43.8 us)
Sparse Core Ops, SparseCore 0:
  12.3 139.5 all-gather.6
  153.6 81.0 all-gather.8
where the time goes:
time: 443 us; the launch traced here: 439 us
  waiting for transfers between devices  136 us (31%)
  starting transfers between devices  95.3 us (22%)
  other arithmetic  94.7 us (21%)
  matrix products  47.9 us (11%)
  blocking collectives  25.5 us (6%)
  local copies, waits for them, and re-layouts  24.6 us (6%)
  between operations  14.4 us (3%)
    all_gather x2, waiting for transfers between devices, in_one_piece(): lax.all_gather(both, axis, axis=dim, tiled=True)  104 us
    another operation x2, other arithmetic, block_terms(): jax.scipy.linalg.solve_triangular(left_side, right_side, lower=True, unit...  79.5 us
    ppermute x16, starting transfers between devices, from_behind(): return lax.ppermute(block, axis, route)  71.1 us
    ppermute x16, waiting for transfers between devices, from_behind(): return lax.ppermute(block, axis, route)  31 us
    all_to_all x1, starting transfers between devices, sent_to_all(): lax.all_to_all(jnp.broadcast_to(x[None], (size, *x.shape)), axis, 0, 0, t...  24.1 us
    all_gather x2, blocking collectives, over_pieces(): return lax.all_gather(x, axis).sum(0)  20.9 us
    dot_general x5, matrix products, on_device(): jnp.dot(normed, piece, preferred_element_type=jnp.float32)  11.8 us
  transfers between devices with their start and end apart: 19, of which 17 were waited for; matrix products, arithmetic and copies ran while one was open for 35% of the time, Pallas kernels for 0%

commit v1 on v0

v1 whole, which is shorter than its diff:
```python
import functools

import jax
import jax.numpy as jnp
from jax import lax
from jax.experimental import pallas as pl
from jax.experimental.pallas import tpu as pltpu
from jax.sharding import PartitionSpec as P

HEADS = 8
HEAD = 128
KSIZE = 31
NX = 4
PAD = 32
EPS = 1e-06
MESH = pl.DeviceIdType.MESH
F32 = jnp.float32
BF16 = jnp.bfloat16


def remote(src, dst, send, recv, **where):
    return pltpu.make_async_remote_copy(
        src_ref=src, dst_ref=dst, send_sem=send, recv_sem=recv, device_id=where, device_id_type=MESH
    )


def arrived(ref, sem):
    pltpu.make_async_copy(ref, ref, sem).wait()


def turn(i, n):
    return lax.rem(i + n, n)


def lanes(i):
    return pl.ds(pl.multiple_of(i * HEAD, HEAD), HEAD)


def composer(z, nz):
    quarter = nz // NX
    return lax.div(z, quarter), lax.rem(z, quarter) == quarter // 2


def gather_kernel(
    nz,
    tok_ref,
    q_ref,
    k_ref,
    v_ref,
    up_ref,
    gate_ref,
    do_ref,
    co_ref,
    gain_ref,
    small_ref,
    spike_ref,
    s0_ref,
    proj_ref,
    raw_ref,
    wout_ref,
    spikes_ref,
    start_ref,
    tok,
    normed,
    win,
    p_send,
    p_recv,
    m_send,
    m_recv,
    t_send,
    t_recv,
    c_send,
    c_recv,
    k_send,
    k_recv,
    s_send,
    s_recv,
    local,
):
    z, x, c = lax.axis_index("sp"), lax.axis_index("fs"), lax.axis_index("tp")
    up, down = turn(z + 1, nz), turn(z - 1, nz)
    right, left, over = turn(x + 1, NX), turn(x - 1, NX), turn(x + 2, NX)
    other = 1 - c
    half = nz // 2
    rows = tok_ref.shape[0]
    seq_me, is_composer = composer(z, nz)

    barrier = pltpu.get_barrier_semaphore()
    for where in ({"sp": up}, {"sp": down}, {"fs": right}, {"fs": left}, {"fs": over}, {"tp": other}):
        pl.semaphore_signal(barrier, inc=1, device_id=where, device_id_type=MESH)
    pl.semaphore_wait(barrier, 6)

    own = [w.at[:, lanes(x)] for w in (q_ref, k_ref, v_ref, up_ref, gate_ref)]
    own += [w.at[lanes(x), :] for w in (do_ref, co_ref)]
    count = len(own)

    def slot(src, j):
        if j < 5:
            return win.at[pl.ds(pl.multiple_of(src * HEAD, HEAD), HEAD), pl.ds(j * HEAD, HEAD)]
        return wout_ref.at[src, j - 5]

    for j in range(count):
        remote(own[j], slot(z, j), p_send.at[0, j], p_recv.at[0, j], sp=up).start()
        remote(own[j], slot(z, j), m_send.at[0, j], m_recv.at[0, j], sp=down).start()

    part = rows // 2
    halves = (pl.ds(0, part), pl.ds(part, part))
    for i in range(2):
        src = tok_ref.at[halves[i]]
        dst = tok.at[x, c, halves[i]]
        remote(src, dst, t_send.at[0, i], t_recv.at[0, i], fs=right).start()
        remote(src, dst, t_send.at[1, i], t_recv.at[1, i], fs=left).start()
    own_over = remote(tok_ref, tok.at[x, c], c_send.at[0], c_recv.at[0], tp=other)
    own_over.start()
    spike_copies = [
        remote(spike_ref, spikes_ref.at[x], k_send.at[d - 1], k_recv.at[d - 1], fs=turn(x + d, NX)) for d in (1, 2, 3)
    ]
    for copy in spike_copies:
        copy.start()
    copies = [
        pltpu.make_async_copy(own[j], slot(z, j), local.at[j]) for j in range(count)
    ]
    copies.append(pltpu.make_async_copy(tok_ref, tok.at[x, c], local.at[count]))
    copies.append(pltpu.make_async_copy(spike_ref, spikes_ref.at[x], local.at[count + 1]))
    for copy in copies:
        copy.start()

    @pl.when(is_composer & (x == seq_me))
    def _():
        sends = [
            remote(s0_ref.at[turn(x + d, NX)], start_ref, s_send.at[d - 1], s_recv.at[0], fs=turn(x + d, NX))
            for d in (1, 2, 3)
        ]
        for copy in sends:
            copy.start()
        mine = pltpu.make_async_copy(s0_ref.at[x], start_ref, local.at[count + 2])
        mine.start()
        mine.wait()
        for copy in sends:
            copy.wait_send()

    @pl.when(jnp.logical_not(is_composer))
    def _():
        start_ref[...] = jnp.zeros_like(start_ref)

    def ring(t, _):
        back, fore = turn(z - t, nz), turn(z + t, nz)
        for j in range(count):
            arrived(slot(back, j), p_recv.at[t - 1, j])

            @pl.when((t < half - 1) | (j % 2 == 0))
            def _(j=j):
                remote(slot(back, j), slot(back, j), p_send.at[t, j], p_recv.at[t, j], sp=up).start()

            arrived(slot(fore, j), m_recv.at[t - 1, j])

            @pl.when((t < half - 1) | (j % 2 == 1))
            def _(j=j):
                remote(slot(fore, j), slot(fore, j), m_send.at[t, j], m_recv.at[t, j], sp=down).start()

        return 0

    first = min(3, half - 1)
    second = min(5, half - 1)
    lax.fori_loop(1, first + 1, ring, 0)
    for i in range(2):
        arrived(tok.at[left, c, halves[i]], t_recv.at[0, i])
        arrived(tok.at[right, c, halves[i]], t_recv.at[1, i])
    remote(tok.at[left, c, halves[0]], tok.at[left, c, halves[0]], t_send.at[2, 0], t_recv.at[2, 0], fs=right).start()
    remote(tok.at[right, c, halves[1]], tok.at[right, c, halves[1]], t_send.at[2, 1], t_recv.at[2, 1], fs=left).start()
    remote(tok.at[left, c], tok.at[left, c], c_send.at[1], c_recv.at[1], tp=other).start()
    remote(tok.at[right, c], tok.at[right, c], c_send.at[2], c_recv.at[2], tp=other).start()
    lax.fori_loop(first + 1, second + 1, ring, 0)
    for i in range(2):
        arrived(tok.at[over, c, halves[i]], t_recv.at[2, i])
    remote(tok.at[over, c], tok.at[over, c], c_send.at[3], c_recv.at[3], tp=other).start()
    copies[count].wait()
    for i, where in enumerate((x, left, right, over)):
        arrived(tok.at[where, other], c_recv.at[i])

    features = tok.shape[-1]
    step = 64

    def norm(i, _):
        s = i // (rows // step)
        r = pl.multiple_of(lax.rem(i, rows // step) * step, step)
        a = tok[s, 0, pl.ds(r, step), :].astype(F32)
        b = tok[s, 1, pl.ds(r, step), :].astype(F32)
        total = jnp.sum(a * a, axis=-1, keepdims=True) + jnp.sum(b * b, axis=-1, keepdims=True)
        scale = lax.rsqrt(total * (1.0 / (2 * features)) + EPS)
        at = pl.ds(pl.multiple_of(i * step, step), step)
        normed[at, :features] = (a * scale * gain_ref[:, :features]).astype(BF16)
        normed[at, features:] = (b * scale * gain_ref[:, features:]).astype(BF16)
        return 0

    lax.fori_loop(0, NX * rows // step, norm, 0)
    lax.fori_loop(second + 1, half, ring, 0)
    far = turn(z + half, nz)
    for j in range(count):
        arrived(slot(far, j), (p_recv if j % 2 == 0 else m_recv).at[half - 1, j])
    for j in range(count):
        copies[j].wait()

    def project(s, _):
        at = pl.ds(pl.multiple_of(s * rows, rows), rows)
        tokens = normed[at, :]
        for lo, hi in ((0, 256), (256, 512), (512, 640)):
            proj_ref[at, lo:hi] = jnp.dot(tokens, win[:, lo:hi], preferred_element_type=F32).astype(BF16)
        raw_ref[at, :] = jnp.dot(tokens, small_ref[...], preferred_element_type=F32).astype(BF16)
        return 0

    lax.fori_loop(0, NX, project, 0)

    @pl.when(is_composer & (x != seq_me))
    def _():
        arrived(start_ref, s_recv.at[0])

    copies[count + 1].wait()
    for d in (1, 2, 3):
        arrived(spikes_ref.at[turn(x - d, NX)], k_recv.at[d - 1])
        spike_copies[d - 1].wait_send()

    def drain(t, _):
        for j in range(count):

            @pl.when((t < half - 1) | (j % 2 == 0))
            def _(j=j):
                remote(slot(z, j), slot(z, j), p_send.at[t, j], p_recv.at[t, j], sp=up).wait_send()

            @pl.when((t < half - 1) | (j % 2 == 1))
            def _(j=j):
                remote(slot(z, j), slot(z, j), m_send.at[t, j], m_recv.at[t, j], sp=down).wait_send()

        return 0

    lax.fori_loop(0, half, drain, 0)
    for i in range(2):
        for where, row in ((right, 0), (left, 1), (right, 2)):
            remote(
                tok.at[x, c, halves[i]], tok.at[x, c, halves[i]], t_send.at[row, i], t_recv.at[row, i], fs=where
            ).wait_send()
    for i in range(4):
        remote(tok.at[x, c], tok.at[x, c], c_send.at[i], c_recv.at[i], tp=other).wait_send()


def gathered(nz, tokens, weights, gain, small, spike, start):
    rows, features = tokens.shape
    half = nz // 2
    count = len(weights)
    vmem = pl.BlockSpec(memory_space=pltpu.VMEM)
    dma = pltpu.SemaphoreType.DMA
    return pl.pallas_call(
        functools.partial(gather_kernel, nz),
        name="gather",
        out_shape=(
            jax.ShapeDtypeStruct((NX * rows, 5 * HEAD), BF16),
            jax.ShapeDtypeStruct((NX * rows, HEAD), BF16),
            jax.ShapeDtypeStruct((nz, 2, HEAD, HEAD), BF16),
            jax.ShapeDtypeStruct((NX, *spike.shape), F32),
            jax.ShapeDtypeStruct((HEAD, HEAD), F32),
        ),
        in_specs=[vmem] * (count + 5),
        out_specs=(vmem,) * 5,
        scratch_shapes=[
            pltpu.VMEM((NX, 2, rows, features), BF16),
            pltpu.VMEM((NX * rows, 2 * features), BF16),
            pltpu.VMEM((nz * HEAD, 5 * HEAD), BF16),
            dma((half, count)),
            dma((half, count)),
            dma((half, count)),
            dma((half, count)),
            dma((3, 2)),
            dma((3, 2)),
            dma((4,)),
            dma((4,)),
            dma((3,)),
            dma((3,)),
            dma((3,)),
            dma((1,)),
            dma((count + 3,)),
        ],
        compiler_params=pltpu.CompilerParams(
            collective_id=0, has_side_effects=True, vmem_limit_bytes=56 * 1024 * 1024
        ),
    )(tokens, *weights, gain, small, spike, start)


def dot(a, b):
    return jnp.dot(a.astype(BF16), b.astype(BF16), preferred_element_type=F32)


def dot_t(a, b):
    dims = (((1,), (1,)), ((), ()))
    return lax.dot_general(a.astype(BF16), b.astype(BF16), dims, preferred_element_type=F32)


def dot_of_t(a, b):
    dims = (((0,), (0,)), ((), ()))
    return lax.dot_general(a.astype(BF16), b.astype(BF16), dims, preferred_element_type=F32)


def silu(a):
    return a * jax.nn.sigmoid(a)


def unit_rows(a):
    return a * lax.rsqrt(jnp.sum(a * a, axis=-1, keepdims=True) + EPS)


def unit_lower_inverse(a, row, col):
    size = a.shape[0]
    eye = jnp.where(row == col, 1.0, 0.0)
    inverse = eye - jnp.where((row - col == 1) & (lax.rem(row, 2) == 1), a, 0.0)
    width = 2
    while width < size:
        same = lax.div(row, 2 * width) == lax.div(col, 2 * width)
        block = jnp.where(same & (lax.div(row, width) != lax.div(col, width)), a, 0.0)
        inverse = inverse - dot(dot(inverse, block), inverse)
        width *= 2
    return inverse


def mix_kernel(
    nz,
    proj_ref,
    raw_ref,
    wpart_ref,
    spikes_ref,
    start_ref,
    rate_ref,
    bias_ref,
    head_gain_ref,
    taps_ref,
    channel_gain_ref,
    out_ref,
    base,
    reader,
    map_out,
    map_in,
    states,
    state_in,
    rim_out,
    rim_in,
    extended,
    conv_out,
    conv_all,
    attn_out,
    attn_all,
    wout,
    partial,
    map_send,
    map_recv,
    state_send,
    state_recv,
    rim_sem,
    conv_send,
    conv_recv,
    attn_send,
    attn_recv,
    w_send,
    w_recv,
):
    z, x, c = lax.axis_index("sp"), lax.axis_index("fs"), lax.axis_index("tp")
    right, left, over = turn(x + 1, NX), turn(x - 1, NX), turn(x + 2, NX)
    other = 1 - c
    head = c * NX + x
    rows = proj_ref.shape[0] // NX
    half = nz // 2
    quarter = nz // NX
    seq_me, is_composer = composer(z, nz)
    last = nz - 1

    barrier = pltpu.get_barrier_semaphore()
    for d in range(1, nz):
        pl.semaphore_signal(barrier, inc=1, device_id={"sp": turn(z + d, nz)}, device_id_type=MESH)
    for d in range(NX):
        peer = turn(x + d, NX)
        if d:
            pl.semaphore_signal(barrier, inc=1, device_id={"fs": peer}, device_id_type=MESH)
        pl.semaphore_signal(barrier, inc=1, device_id={"fs": peer, "tp": other}, device_id_type=MESH)

    rate = jnp.exp(jnp.full((1, rows), rate_ref[head], F32))
    bias = bias_ref[head]
    row = lax.broadcasted_iota(jnp.int32, (rows, rows), 0)
    col = lax.broadcasted_iota(jnp.int32, (rows, rows), 1)

    for s in range(NX):
        at = pl.ds(s * rows, rows)
        glu = proj_ref[at, 384:512].astype(F32) * jax.nn.sigmoid(proj_ref[at, 512:640].astype(F32))
        glu = glu.astype(BF16)
        extended[s, pl.ds(PAD, rows), :] = glu.astype(F32)
        rim_out[s] = glu[rows - PAD :]

    def delta(s):
        at = pl.ds(s * rows, rows)
        query = unit_rows(silu(proj_ref[at, 0:128].astype(F32))) * HEAD ** (-0.5)
        keys = unit_rows(silu(proj_ref[at, 128:256].astype(F32)))
        values = silu(proj_ref[at, 256:384].astype(F32))
        raw = raw_ref[at, :]
        pick = lax.broadcasted_iota(jnp.int32, (8, HEAD), 1) == head
        logit = dot_t(jnp.where(pick, 1.0, 0.0), raw)[0:1]
        soft = jnp.maximum(logit, 0.0) + jnp.log1p(jnp.exp(-jnp.abs(logit)))
        log_row = -rate * soft + spikes_ref[s, pl.ds(x, 1), :]
        place = lax.broadcasted_iota(jnp.int32, (rows, HEAD), 1) == HEADS + head
        beta = jnp.sum(jnp.where(place, raw.astype(F32), 0.0), axis=1, keepdims=True)
        beta = jax.nn.sigmoid(beta + bias)
        log_col = jnp.sum(jnp.where(row == col, log_row, 0.0), axis=1, keepdims=True)
        cum_col = jnp.sum(jnp.where(col <= row, log_row, 0.0), axis=1, keepdims=True)
        cum_row = jnp.sum(jnp.where(row <= col, log_col, 0.0), axis=0, keepdims=True)
        total = cum_col[rows - 1 :, :]
        gamma = jnp.where(col <= row, jnp.exp(jnp.minimum(cum_col - cum_row, 0.0)), 0.0)
        grown = jnp.exp(cum_col)
        gram = dot_t(keys, keys)
        a_matrix = jnp.where(col < row, beta * gram * gamma, 0.0)
        inverse = unit_lower_inverse(a_matrix, row, col)
        both = dot(inverse, jnp.concatenate([beta * values, (beta * grown) * keys], axis=1))
        decayed = keys * jnp.exp(total - cum_col)
        mapped = dot_of_t(decayed, both)
        keep = jnp.exp(total)
        keep_hi = keep.astype(BF16).astype(F32)
        rest = keep - keep_hi
        tail = lax.broadcasted_iota(jnp.int32, (16, 2 * HEAD), 0)
        map_out[s, 0:HEAD, :] = mapped.astype(BF16)
        map_out[s, HEAD:, :] = jnp.where(tail < 8, keep_hi, rest).astype(BF16)
        scores = dot_t(query, keys) * gamma
        read = dot(scores, both)
        base[s] = read[:, :HEAD]
        reader[s] = (grown * query - read[:, HEAD:]).astype(BF16)

    def send_map(s):
        owner = s * quarter + quarter // 2

        @pl.when((z != owner) & (z != last))
        def _():
            remote(map_out.at[s], map_in.at[z], map_send.at[s], map_recv.at[z], sp=owner).start()

        @pl.when((z == owner) & (z != last))
        def _():
            pltpu.make_async_copy(map_out.at[s], map_in.at[z], map_recv.at[z]).start()

    delta(0)
    pl.semaphore_wait(barrier, last + 2 * NX - 1)

    @pl.when(z < last)
    def _():
        remote(rim_out, rim_in, rim_sem.at[0], rim_sem.at[1], sp=z + 1).start()

    mine = wpart_ref.at[pl.ds(c * half, half)]
    theirs = wpart_ref.at[pl.ds(other * half, half)]
    own_w = pltpu.make_async_copy(mine, wout.at[head], w_recv.at[9])
    first_w = [
        remote(mine, wout.at[head], w_send.at[0], w_recv.at[0], fs=right),
        remote(theirs, wout.at[head], w_send.at[1], w_recv.at[1], fs=right, tp=other),
        remote(mine, wout.at[head], w_send.at[2], w_recv.at[2], fs=left),
        remote(theirs, wout.at[head], w_send.at[3], w_recv.at[3], fs=left, tp=other),
        remote(theirs, wout.at[head], w_send.at[4], w_recv.at[4], tp=other),
    ]
    own_w.start()
    for copy in first_w:
        copy.start()
    for s in range(1, NX):
        delta(s)
        send_map(s - 1)

    @pl.when(z > 0)
    def _():
        arrived(rim_in, rim_sem.at[1])
        extended[:, 0:PAD, :] = rim_in[...].astype(F32)

    @pl.when(z == 0)
    def _():
        extended[:, 0:PAD, :] = jnp.zeros((NX, PAD, HEAD), F32)

    send_map(NX - 1)

    piece = 64
    pieces = rows // piece
    taps = taps_ref[:, lanes(head)]

    for s in range(NX):
        for r in range(pieces):
            conv = jnp.zeros((piece, HEAD), F32)
            for tap in range(KSIZE):
                conv = conv + taps[tap : tap + 1] * extended[s, pl.ds(r * piece + tap + PAD - KSIZE + 1, piece), :]
            conv_out[s, pl.ds(r * piece, piece), :] = conv.astype(BF16)

    @pl.when(is_composer)
    def _():

        def give(i):
            @pl.when(i != z)
            def _():
                remote(states.at[i], state_in.at[seq_me], state_send.at[i], state_recv.at[seq_me], sp=i).start()

            @pl.when(i == z)
            def _():
                pltpu.make_async_copy(states.at[i], state_in.at[seq_me], state_recv.at[seq_me]).start()

        def advance(i, state):
            states[i] = state.astype(BF16)
            arrived(map_in.at[i], map_recv.at[i])
            block = map_in[i]
            keep = block[HEAD : HEAD + 1, :HEAD].astype(F32) + block[HEAD + 8 : HEAD + 9, :HEAD].astype(F32)
            high = state.astype(BF16)
            low = state - high.astype(F32)
            reduce = dot(block[:HEAD, HEAD:], high) + dot(block[:HEAD, HEAD:], low)
            result = keep * state - reduce + block[:HEAD, :HEAD].astype(F32)
            give(i)
            return result

        states[last] = lax.fori_loop(0, last, advance, start_ref[...]).astype(BF16)

    def exchange(src, dst, send, recv):
        for d in range(NX):
            s = turn(x + d, NX)
            if d == 0:
                pltpu.make_async_copy(src.at[s], dst.at[:, lanes(head)], recv.at[0]).start()
            else:
                remote(src.at[s], dst.at[:, lanes(head)], send.at[d], recv.at[d], fs=s).start()
            remote(src.at[s], dst.at[:, lanes(head)], send.at[NX + d], recv.at[NX + d], fs=s, tp=other).start()

    def exchanged(src, dst, send, recv):
        for d in range(NX):
            source = turn(x - d, NX)
            arrived(dst.at[:, lanes(c * NX + source)], recv.at[d])
            arrived(dst.at[:, lanes(other * NX + source)], recv.at[NX + d])
            if d:
                remote(src.at[0], dst.at[:, lanes(head)], send.at[d], recv.at[d], fs=right).wait_send()
            remote(src.at[0], dst.at[:, lanes(head)], send.at[NX + d], recv.at[NX + d], fs=right).wait_send()

    exchange(conv_out, conv_all, conv_send, conv_recv)

    @pl.when(is_composer)
    def _():
        @pl.when(z != last)
        def _():
            remote(states.at[last], state_in.at[seq_me], state_send.at[last], state_recv.at[seq_me], sp=last).start()

        @pl.when(z == last)
        def _():
            pltpu.make_async_copy(states.at[last], state_in.at[seq_me], state_recv.at[seq_me]).start()

    w_arrivals = ((c, left, 0), (other, left, 1), (c, right, 2), (other, right, 3))
    near, rest = pl.ds(0, half // 2), pl.ds(half // 2, half - half // 2)
    for core, source, i in w_arrivals:
        held = wout.at[core * NX + source]
        arrived(held, w_recv.at[i])
        part = held.at[near] if i < 2 else held.at[rest]
        remote(part, part, w_send.at[5 + i], w_recv.at[5 + i], fs=right if i < 2 else left).start()

    head_gain = head_gain_ref[...]
    for s in range(NX):
        arrived(state_in.at[s], state_recv.at[s])
        attn = base[s] + jnp.dot(reader[s], state_in[s], preferred_element_type=F32)
        scale = lax.rsqrt(jnp.mean(attn * attn, axis=-1, keepdims=True) + EPS)
        attn_out[s] = (attn * scale * head_gain).astype(BF16)

    exchange(attn_out, attn_all, attn_send, attn_recv)
    exchanged(conv_out, conv_all, conv_send, conv_recv)

    def channel_norm(i, _):
        at = pl.ds(pl.multiple_of(i * 64, 64), 64)
        conv = conv_all[at, :].astype(F32)
        mean = jnp.mean(conv, axis=-1, keepdims=True)
        var = jnp.mean(conv * conv, axis=-1, keepdims=True) - mean * mean
        conv_all[at, :] = silu((conv - mean) * lax.rsqrt(var + EPS) * channel_gain_ref[...]).astype(BF16)
        return 0

    lax.fori_loop(0, rows // 64, channel_norm, 0)
    arrived(wout.at[head], w_recv.at[9])
    arrived(wout.at[other * NX + x], w_recv.at[4])
    for core, i in ((c, 5), (other, 6), (c, 7), (other, 8)):
        held = wout.at[core * NX + over]
        arrived(held.at[near] if i < 7 else held.at[rest], w_recv.at[i])

    def weights(j, kind):
        return wout[:, j, kind].reshape(HEADS * HEAD, HEAD)

    def conv_part(j, _):
        partial[j] = jnp.dot(conv_all[...], weights(j, 1), preferred_element_type=F32)
        return 0

    lax.fori_loop(0, half, conv_part, 0)
    exchanged(attn_out, attn_all, attn_send, attn_recv)

    def attn_part(j, _):
        total = partial[j] + jnp.dot(attn_all[...], weights(j, 0), preferred_element_type=F32)
        out_ref[:, lanes(j)] = total.astype(BF16)
        return 0

    lax.fori_loop(0, half, attn_part, 0)

    for s in range(NX):

        @pl.when((z != s * quarter + quarter // 2) & (z != last))
        def _(s=s):
            remote(map_out.at[s], map_in.at[z], map_send.at[s], map_recv.at[z], sp=0).wait_send()

    @pl.when(z < last)
    def _():
        remote(rim_out, rim_in, rim_sem.at[0], rim_sem.at[1], sp=z + 1).wait_send()

    @pl.when(is_composer)
    def _():
        def drain(i, _):
            @pl.when(i != z)
            def _():
                remote(states.at[i], state_in.at[seq_me], state_send.at[i], state_recv.at[seq_me], sp=i).wait_send()

            return 0

        lax.fori_loop(0, nz, drain, 0)

    for copy in first_w:
        copy.wait_send()
    for core, source, i in w_arrivals:
        held = wout.at[core * NX + source]
        part = held.at[near] if i < 2 else held.at[rest]
        remote(part, part, w_send.at[5 + i], w_recv.at[5 + i], fs=right).wait_send()


def mixed_tokens(nz, rows, proj, raw, wpart, spikes, start, rate, bias, head_gain, taps, channel_gain):
    half = nz // 2
    vmem = pl.BlockSpec(memory_space=pltpu.VMEM)
    smem = pl.BlockSpec(memory_space=pltpu.SMEM)
    dma = pltpu.SemaphoreType.DMA
    width = HEADS * HEAD
    return pl.pallas_call(
        functools.partial(mix_kernel, nz),
        name="mix",
        out_shape=jax.ShapeDtypeStruct((rows, half * HEAD), BF16),
        in_specs=[vmem] * 5 + [smem] * 2 + [vmem] * 3,
        out_specs=vmem,
        scratch_shapes=[
            pltpu.VMEM((NX, rows, HEAD), F32),
            pltpu.VMEM((NX, rows, HEAD), BF16),
            pltpu.VMEM((NX, HEAD + 16, 2 * HEAD), BF16),
            pltpu.VMEM((nz, HEAD + 16, 2 * HEAD), BF16),
            pltpu.VMEM((nz, HEAD, HEAD), BF16),
            pltpu.VMEM((NX, HEAD, HEAD), BF16),
            pltpu.VMEM((NX, PAD, HEAD), BF16),
            pltpu.VMEM((NX, PAD, HEAD), BF16),
            pltpu.VMEM((NX, PAD + rows, HEAD), F32),
            pltpu.VMEM((NX, rows, HEAD), BF16),
            pltpu.VMEM((rows, width), BF16),
            pltpu.VMEM((NX, rows, HEAD), BF16),
            pltpu.VMEM((rows, width), BF16),
            pltpu.VMEM((HEADS, half, 2, HEAD, HEAD), BF16),
            pltpu.VMEM((half, rows, HEAD), F32),
            dma((NX,)),
            dma((nz,)),
            dma((nz,)),
            dma((NX,)),
            dma((2,)),
            dma((2 * NX,)),
            dma((2 * NX,)),
            dma((2 * NX,)),
            dma((2 * NX,)),
            dma((9,)),
            dma((10,)),
        ],
        compiler_params=pltpu.CompilerParams(
            collective_id=1, has_side_effects=True, vmem_limit_bytes=56 * 1024 * 1024
        ),
    )(proj, raw, wpart, spikes, start, rate, bias, head_gain, taps, channel_gain)


def on_device(
    nz,
    tokens,
    input_norm_gain,
    query_weight,
    key_weight,
    value_weight,
    decay_gate_weight,
    write_strength_weight,
    up_weight,
    gate_half_weight,
    log_decay_rate,
    write_strength_bias,
    decay_spike_added,
    starting_state,
    head_norm_gain,
    convolution_kernel,
    channel_norm_gain,
    delta_output_rows,
    convolution_output_rows,
):
    rows = tokens.shape[1]
    small = jnp.concatenate([decay_gate_weight, write_strength_weight], axis=1)
    small = jnp.pad(small, ((0, 0), (0, HEAD - small.shape[1])))
    spike = jnp.pad(decay_spike_added[0].T, ((0, 8 - NX), (0, 0)))
    weights = (
        query_weight,
        key_weight,
        value_weight,
        up_weight,
        gate_half_weight,
        delta_output_rows,
        convolution_output_rows,
    )
    proj, raw, wpart, spikes, start = gathered(
        nz, tokens[0], weights, input_norm_gain[None], small, spike, starting_state[0]
    )
    mixed = mixed_tokens(
        nz,
        rows,
        proj,
        raw,
        wpart,
        spikes,
        start,
        log_decay_rate,
        write_strength_bias,
        head_norm_gain[None],
        convolution_kernel,
        channel_norm_gain[None],
    )
    return mixed[None]


def solution(mesh):
    return jax.shard_map(
        functools.partial(on_device, mesh.shape["sp"]),
        mesh=mesh,
        in_specs=(
            P(("grp", "fs"), "sp", "tp"),
            P(),
            P("sp", "tp"),
            P("sp", "tp"),
            P("sp", "tp"),
            P(),
            P(),
            P("sp", "tp"),
            P("sp", "tp"),
            P(),
            P(),
            P(("grp", "fs"), "sp", "tp"),
            P(("grp", "fs"), "tp", None, None),
            P(),
            P(),
            P(),
            P("tp", "sp"),
            P("tp", "sp"),
        ),
        out_specs=P(("grp", "fs"), "sp", "tp"),
        check_vma=False,
    )
```

time: 443 us -> 147 us (0.33)
  Pallas kernels: 0 us -> 141 us
  waiting for transfers between devices: 136 us -> 0 us
  starting transfers between devices: 95.3 us -> 0 us
  other arithmetic: 94.7 us -> 0.78 us
  matrix products: 47.9 us -> 0 us
  blocking collectives: 25.5 us -> 0 us
  local copies, waits for them, and re-layouts: 24.6 us -> 4.32 us
  between operations: 14.4 us -> 0.03 us
    pallas_call x0 -> x2, Pallas kernels: none -> 141 us  [the longest x1 81.2 us: gathered(): pl.pallas_call(functools.partial(gather_kernel, nz), name='gather', out_s...]
    all_gather x2 -> x0, waiting for transfers between devices: 104 us -> none  [in_one_piece(): lax.all_gather(both, axis, axis=dim, tiled=True)]
    another operation x3 -> x0, other arithmetic: 80.5 us -> none  [the longest x2 79.5 us: block_terms(): jax.scipy.linalg.solve_triangular(left_side, right_side, lower=True, unit...]
    ppermute x16 -> x0, starting transfers between devices: 71.1 us -> none  [from_behind(): return lax.ppermute(block, axis, route)]
    dot_general x57 -> x0, matrix products: 46.8 us -> none  [the longest x5 11.8 us: on_device(): jnp.dot(normed, piece, preferred_element_type=jnp.float32)]
    ppermute x16 -> x0, waiting for transfers between devices: 31 us -> none  [from_behind(): return lax.ppermute(block, axis, route)]
    all_to_all x1 -> x0, starting transfers between devices: 24.1 us -> none  [sent_to_all(): lax.all_to_all(jnp.broadcast_to(x[None], (size, *x.shape)), axis, 0, 0, t...]
    all_gather x2 -> x0, blocking collectives: 20.9 us -> none  [over_pieces(): return lax.all_gather(x, axis).sum(0)]
  transfers between devices with their start and end apart: 19 -> 0, of which waited for: 17 -> 0; matrix products, arithmetic and copies ran while one was open for 35% -> 0% of each run, Pallas kernels for 0% -> 0%
where the time goes in v1:
time: 147 us; the launch traced here: 146 us
  Pallas kernels  141 us (96%)
  local copies, waits for them, and re-layouts  4.32 us (3%)
    pallas_call x1, Pallas kernels, gathered(): pl.pallas_call(functools.partial(gather_kernel, nz), name='gather', out_s...  81.2 us
    pallas_call x1, Pallas kernels, mixed_tokens(): pl.pallas_call(functools.partial(mix_kernel, nz), name='mix', out_shape=j...  59.9 us

profile of v1, /device:TPU:33, one launch (start us, length us, event | category | flops | bytes accessed | tf_op | source)
XLA Modules:
  0.0 146.2 jit_solution(12174362415596189071)
XLA Ops:
  0.0 1.3 pad.9.spike_ref
  1.3 0.8 pad_maximum_fusion
  2.1 0.3 copy.21
  2.3 0.9 pad.8.small_ref
  3.2 81.2 %gather.1 = (bf16[1024,640]{1,0:T(8,128)(2,1)}, bf16[1024,128]{1,0:T(8,128)(2,1)}, bf16[16,2,128,128]{3,2,1,0:T(8,128)(2,1)}, f32[4,8,256]{2,1,0:T(8,128)}, f32[128,128]{1,0:T(8,128)}) custom-call(bf16[256,1024]{1,0:T(8,128)(2,1)} %bitcast.10, bf16[128,512]{1,0:T(8,128)(2,1)} %q_ref.1, bf16[128,512]{1,0:T(8,128)(2,1)} %k_ref.1, bf16[128,512]{1,0:T(8,128)(2,1)} %v_ref.1, ...), custom_call_target="tpu_custom_call" | custom-call | tf_op jit(solution)/shard_map/gather/pallas_call | solution.py:252
  84.5 59.9 %mix.1 = bf16[256,1024]{1,0:T(8,128)(2,1)} custom-call(bf16[1024,640]{1,0:T(8,128)(2,1)} %get-tuple-element.10.proj_ref, bf16[1024,128]{1,0:T(8,128)(2,1)} %get-tuple-element.11.raw_ref, bf16[16,2,128,128]{3,2,1,0:T(8,128)(2,1)} %get-tuple-element.12.wpart_ref, f32[4,8,256]{2,1,0:T(8,128)} %get-tuple-element.13.spikes_ref, ...), custom_call_target="tpu_custom_call" | custom-call | tf_op jit(solution)/shard_map/mix/pallas_call | solution.py:628
  144.4 1.9 %copy.23 = bf16[1,256,1024]{2,1,0:T(8,128)(2,1)} copy(bf16[1,256,1024]{2,1,0:T(8,128)(2,1)} %bitcast.9) | data formatting | bytes 1048576

commit v2 on v1

v2 whole, which is shorter than its diff:
```python
import functools

import jax
import jax.numpy as jnp
from jax import lax
from jax.experimental import pallas as pl
from jax.experimental.pallas import tpu as pltpu
from jax.sharding import PartitionSpec as P

HEADS = 8
HEAD = 128
KSIZE = 31
NX = 4
PAD = 32
EPS = 1e-06
MESH = pl.DeviceIdType.MESH
F32 = jnp.float32
BF16 = jnp.bfloat16


def remote(src, dst, send, recv, **where):
    return pltpu.make_async_remote_copy(
        src_ref=src, dst_ref=dst, send_sem=send, recv_sem=recv, device_id=where, device_id_type=MESH
    )


def arrived(ref, sem):
    pltpu.make_async_copy(ref, ref, sem).wait()


def turn(i, n):
    return lax.rem(i + n, n)


def lanes(i):
    return pl.ds(pl.multiple_of(i * HEAD, HEAD), HEAD)


def composer(z, nz):
    quarter = nz // NX
    return lax.div(z, quarter), lax.rem(z, quarter) == quarter // 2


def dot(a, b):
    return jnp.dot(a.astype(BF16), b.astype(BF16), preferred_element_type=F32)


def dot_t(a, b):
    dims = (((1,), (1,)), ((), ()))
    return lax.dot_general(a.astype(BF16), b.astype(BF16), dims, preferred_element_type=F32)


def dot_of_t(a, b):
    dims = (((0,), (0,)), ((), ()))
    return lax.dot_general(a.astype(BF16), b.astype(BF16), dims, preferred_element_type=F32)


def silu(a):
    return a * jax.nn.sigmoid(a)


def unit_rows(a):
    return a * lax.rsqrt(jnp.sum(a * a, axis=-1, keepdims=True) + EPS)


def unit_lower_inverse(a, row, col):
    size = a.shape[0]
    eye = jnp.where(row == col, 1.0, 0.0)
    inverse = eye - jnp.where((row - col == 1) & (lax.rem(row, 2) == 1), a, 0.0)
    width = 2
    while width < size:
        same = lax.div(row, 2 * width) == lax.div(col, 2 * width)
        block = jnp.where(same & (lax.div(row, width) != lax.div(col, width)), a, 0.0)
        inverse = inverse - dot(dot(inverse, block), inverse)
        width *= 2
    return inverse


def kernel(
    nz,
    paired,
    tok_ref,
    k_ref,
    v_ref,
    q_ref,
    up_ref,
    gate_ref,
    do_ref,
    co_ref,
    gain_ref,
    decay_ref,
    strength_ref,
    spike_ref,
    s0_ref,
    rate_ref,
    bias_ref,
    head_gain_ref,
    taps_ref,
    channel_gain_ref,
    out_ref,
    tok,
    normed,
    win,
    wring,
    wout,
    spike_rows,
    spikes,
    start,
    keys_at,
    gammas,
    growth,
    solved,
    base,
    reader,
    map_out,
    map_in,
    states,
    state_in,
    rim_out,
    rim_in,
    extended,
    conv_out,
    conv_all,
    attn_out,
    attn_all,
    partial,
    ring_send,
    ring_recv,
    y_send,
    y_recv,
    near_send,
    near_recv,
    far_send,
    far_recv,
    own_send,
    own_recv,
    t_send,
    t_recv,
    c_send,
    c_recv,
    k_send,
    k_recv,
    s_send,
    s_recv,
    local,
    map_send,
    map_recv,
    state_send,
    state_recv,
    rim_sem,
    conv_send,
    conv_recv,
    attn_send,
    attn_recv,
):
    z, x, c = lax.axis_index("sp"), lax.axis_index("fs"), lax.axis_index("tp")
    up, down = turn(z + 1, nz), turn(z - 1, nz)
    right, left, over = turn(x + 1, NX), turn(x - 1, NX), turn(x + 2, NX)
    other = 1 - c
    head = c * NX + x
    half = nz // 2
    quarter = nz // NX
    last = nz - 1
    rows, features = tok_ref.shape
    seq_me, is_composer = composer(z, nz)
    group = lax.axis_index("grp")
    parity = lax.rem(group, 2)
    partner = group + 1 - 2 * parity

    neighbours = [{"sp": up}, {"sp": down}, {"fs": right}, {"fs": left}, {"fs": over}, {"tp": other}]
    neighbours += [{"fs": right, "tp": other}, {"fs": left, "tp": other}, {"fs": over, "tp": other}]
    if paired:
        neighbours.append({"grp": partner})
    barrier = pltpu.get_barrier_semaphore()
    for where in neighbours:
        pl.semaphore_signal(barrier, inc=1, device_id=where, device_id_type=MESH)

    def block_of(src, j):
        return win.at[pl.ds(pl.multiple_of(src * HEAD, HEAD), HEAD), lanes(j)]

    own = [w.at[:, lanes(x)] for w in (k_ref, v_ref, q_ref, up_ref, gate_ref)]
    own += [w.at[lanes(x), :] for w in (do_ref, co_ref)]
    own_at = [block_of(z, j) for j in range(5)] + [wring.at[z, j] for j in range(2)]
    copies = [pltpu.make_async_copy(a, b, local.at[j]) for j, (a, b) in enumerate(zip(own, own_at))]
    copies.append(pltpu.make_async_copy(tok_ref, tok.at[x, c], local.at[7]))
    for copy in copies:
        copy.start()

    row = lax.broadcasted_iota(jnp.int32, (rows, rows), 0)
    col = lax.broadcasted_iota(jnp.int32, (rows, rows), 1)

    def to_row(column):
        return jnp.sum(jnp.where(row == col, column, 0.0), axis=0, keepdims=True)

    def to_column(line):
        return jnp.sum(jnp.where(row == col, line, 0.0), axis=1, keepdims=True)

    spike = spike_ref[...]
    spike_rows[...] = jnp.zeros_like(spike_rows)
    for i in range(NX):
        spike_rows[i : i + 1, :] = to_row(spike[:, i : i + 1])

    if paired:
        places = [lambda src, j=j: block_of(src, j) for j in range(3)]
        places += [lambda src: block_of(src, 3 + parity), lambda src: wring.at[src, parity]]
        shared = {3: 0, 4: 1}
    else:
        places = [lambda src, j=j: block_of(src, j) for j in range(5)]
        places += [lambda src, j=j: wring.at[src, j] for j in range(2)]
        shared = {}
    count = len(places)

    def hop(t, pos, way, src):
        ref = places[pos](src)
        sem = ring_send.at[way, lax.rem(t, 2), pos]
        return remote(ref, ref, sem, ring_recv.at[way, t, pos], sp=up if way == 0 else down)

    def spread(src):
        core, zz = lax.div(src, half), lax.rem(src, half)
        other_core = core + c - 2 * core * c
        piece, target = wring.at[src], wout.at[head, zz]
        remote(piece, target, near_send.at[0, src], near_recv.at[0, other_core, zz], fs=right, tp=core).start()
        remote(piece, target, near_send.at[1, src], near_recv.at[1, other_core, zz], fs=left, tp=core).start()

        @pl.when(other_core == 0)
        def _():
            pltpu.make_async_copy(piece, target, own_recv.at[0, zz]).start()

        @pl.when(other_core == 1)
        def _():
            remote(piece, target, own_send.at[zz], own_recv.at[1, zz], tp=other).start()

    pl.semaphore_wait(barrier, len(neighbours))
    for j in range(7):
        copies[j].wait()
    for pos in range(count):
        hop(0, pos, 0, z).start()
        hop(0, pos, 1, z).start()

    part = rows // 2
    halves = (pl.ds(0, part), pl.ds(part, part))
    for i in range(2):
        src = tok_ref.at[halves[i]]
        dst = tok.at[x, c, halves[i]]
        remote(src, dst, t_send.at[0, i], t_recv.at[0, i], fs=right).start()
        remote(src, dst, t_send.at[1, i], t_recv.at[1, i], fs=left).start()
    remote(tok_ref, tok.at[x, c], c_send.at[0], c_recv.at[0], tp=other).start()
    spike_copies = [
        remote(spike_rows, spikes.at[x], k_send.at[d - 1], k_recv.at[d - 1], fs=turn(x + d, NX)) for d in (1, 2, 3)
    ]
    for copy in spike_copies:
        copy.start()
    spike_own = pltpu.make_async_copy(spike_rows, spikes.at[x], local.at[8])
    spike_own.start()

    start_sends = [
        remote(s0_ref.at[turn(x + d, NX)], start, s_send.at[d - 1], s_recv.at[0], fs=turn(x + d, NX)) for d in (1, 2, 3)
    ]

    @pl.when(is_composer & (x == seq_me))
    def _():
        for copy in start_sends:
            copy.start()
        pltpu.make_async_copy(s0_ref.at[x], start, s_recv.at[0]).start()

    spread(z)

    step = 64

    def norm(s):
        def some(i, _):
            r = pl.ds(pl.multiple_of(i * step, step), step)
            a = tok[s, 0, r, :].astype(F32)
            b = tok[s, 1, r, :].astype(F32)
            total = jnp.sum(a * a, axis=-1, keepdims=True) + jnp.sum(b * b, axis=-1, keepdims=True)
            scale = lax.rsqrt(total * (1.0 / (2 * features)) + EPS)
            at = pl.ds(pl.multiple_of(s * rows + i * step, step), step)
            normed[at, :features] = (a * scale * gain_ref[:, :features]).astype(BF16)
            normed[at, features:] = (b * scale * gain_ref[:, features:]).astype(BF16)
            return 0

        lax.fori_loop(0, rows // step, some, 0)

    def pass_on(i, src):
        remote(tok.at[src, c], tok.at[src, c], c_send.at[i], c_recv.at[i], tp=other).start()

    def tokens_near():
        for i in range(2):
            arrived(tok.at[left, c, halves[i]], t_recv.at[0, i])
            arrived(tok.at[right, c, halves[i]], t_recv.at[1, i])
        a, b = tok.at[left, c, halves[0]], tok.at[right, c, halves[1]]
        remote(a, a, t_send.at[2, 0], t_recv.at[2, 0], fs=right).start()
        remote(b, b, t_send.at[2, 1], t_recv.at[2, 1], fs=left).start()
        pass_on(1, left)
        pass_on(2, right)

    def norm_own():
        copies[7].wait()
        arrived(tok.at[x, other], c_recv.at[0])
        norm(x)

    def norm_near(i, src):
        arrived(tok.at[src, other], c_recv.at[i])
        norm(src)

    def tokens_far():
        for i in range(2):
            arrived(tok.at[over, c, halves[i]], t_recv.at[2, i])
        pass_on(3, over)

    hooks = (
        (2, norm_own),
        (4, tokens_near),
        (5, lambda: norm_near(1, left)),
        (6, lambda: norm_near(2, right)),
        (6, tokens_far),
    )

    def ring(t, _):
        back, fore = turn(z - t, nz), turn(z + t, nz)
        for pos in range(count):
            for way, src in ((0, back), (1, fore)):
                arrived(places[pos](src), ring_recv.at[way, t - 1, pos])

                @pl.when(t >= 2)
                def _(pos=pos, way=way):
                    hop(t, pos, way, z).wait_send()

                @pl.when((t < half - 1) | (pos % 2 == way))
                def _(pos=pos, way=way, src=src):
                    hop(t, pos, way, src).start()

                if pos in shared:
                    ref = places[pos](src)
                    i = shared[pos]
                    remote(ref, ref, y_send.at[src, i], y_recv.at[src, i], grp=partner).start()

        @pl.when(t >= 2)
        def _():
            for src in (turn(z - t + 1, nz), turn(z + t - 1, nz)):
                if paired:
                    arrived(wring.at[src, 1 - parity], y_recv.at[src, 1])
                spread(src)

        for when, task in hooks:
            pl.when(t == min(when, half - 1))(task)
        return 0

    lax.fori_loop(1, half, ring, 0)
    far = turn(z + half, nz)
    for pos in range(count):
        arrived(places[pos](far), ring_recv.at[pos % 2, half - 1, pos])
        if pos in shared:
            ref = places[pos](far)
            i = shared[pos]
            remote(ref, ref, y_send.at[far, i], y_recv.at[far, i], grp=partner).start()
    norm_near(3, over)

    for d in (1, 2, 3):
        arrived(spikes.at[turn(x - d, NX)], k_recv.at[d - 1])
    spike_own.wait()

    rate = jnp.exp(jnp.full((rows, 1), rate_ref[head], F32))
    bias = bias_ref[head]
    lane = lax.broadcasted_iota(jnp.int32, (rows, HEADS), 1)

    def delta(s):
        at = pl.ds(s * rows, rows)
        tokens = normed[at, :]
        raw = jnp.dot(tokens, win[:, : 2 * HEAD], preferred_element_type=F32).astype(BF16).astype(F32)
        keys = unit_rows(silu(raw[:, :HEAD]))
        values = silu(raw[:, HEAD:])

        def gate(ref):
            both = jnp.dot(tokens, ref[...], preferred_element_type=F32).astype(BF16).astype(F32)
            return jnp.sum(jnp.where(lane == head, both, 0.0), axis=1, keepdims=True)

        logit = gate(decay_ref)
        beta = jax.nn.sigmoid(gate(strength_ref) + bias)
        soft = jnp.maximum(logit, 0.0) + jnp.log1p(jnp.exp(-jnp.abs(logit)))
        log_col = to_column(spikes[s, pl.ds(x, 1), :]) - rate * soft
        log_row = to_row(log_col)
        cum_col = jnp.sum(jnp.where(col <= row, log_row, 0.0), axis=1, keepdims=True)
        cum_row = jnp.sum(jnp.where(row <= col, log_col, 0.0), axis=0, keepdims=True)
        total = cum_col[rows - 1 :, :]
        gamma = jnp.where(col <= row, jnp.exp(jnp.minimum(cum_col - cum_row, 0.0)), 0.0)
        grown = jnp.exp(cum_col)
        a_matrix = jnp.where(col < row, beta * dot_t(keys, keys) * gamma, 0.0)
        inverse = unit_lower_inverse(a_matrix, row, col)
        both = dot(inverse, jnp.concatenate([beta * values, (beta * grown) * keys], axis=1)).astype(BF16)
        mapped = dot_of_t(keys * jnp.exp(total - cum_col), both)
        keep = jnp.exp(total)
        keep_hi = keep.astype(BF16).astype(F32)
        tail = lax.broadcasted_iota(jnp.int32, (16, 2 * HEAD), 0)
        map_out[s, 0:HEAD, :] = mapped.astype(BF16)
        map_out[s, HEAD:, :] = jnp.where(tail < 8, keep_hi, keep - keep_hi).astype(BF16)
        keys_at[s] = keys.astype(BF16)
        gammas[s] = gamma
        growth[s] = jnp.broadcast_to(grown, (rows, HEAD))
        solved[s] = both

    def send_map(s):
        owner = s * quarter + quarter // 2

        @pl.when((z != owner) & (z != last))
        def _():
            remote(map_out.at[s], map_in.at[z], map_send.at[s], map_recv.at[z], sp=owner).start()

        @pl.when((z == owner) & (z != last))
        def _():
            pltpu.make_async_copy(map_out.at[s], map_in.at[z], map_recv.at[z]).start()

    for s in range(NX):
        delta(s)
        if s:
            send_map(s - 1)

    for src in (turn(z - half + 1, nz), turn(z + half - 1, nz), far):
        if paired:
            arrived(wring.at[src, 1 - parity], y_recv.at[src, 1])
        spread(src)
    send_map(NX - 1)
    if paired:

        def shared_in(d, _):
            src = turn(z + d, nz)
            arrived(block_of(src, 4 - parity), y_recv.at[src, 0])
            return 0

        lax.fori_loop(1, nz, shared_in, 0)

    def gated(s):
        at = pl.ds(s * rows, rows)
        raw = jnp.dot(normed[at, :], win[:, 3 * HEAD :], preferred_element_type=F32).astype(BF16).astype(F32)
        glu = (raw[:, :HEAD] * jax.nn.sigmoid(raw[:, HEAD:])).astype(BF16)
        extended[s, pl.ds(PAD, rows), :] = glu.astype(F32)
        rim_out[s] = glu[rows - PAD :]

    def reads(s):
        at = pl.ds(s * rows, rows)
        raw = jnp.dot(normed[at, :], win[:, 2 * HEAD : 3 * HEAD], preferred_element_type=F32).astype(BF16).astype(F32)
        query = unit_rows(silu(raw)) * HEAD ** (-0.5)
        scores = dot_t(query, keys_at[s]) * gammas[s]
        read = dot(scores, solved[s])
        base[s] = read[:, :HEAD]
        reader[s] = (growth[s] * query - read[:, HEAD:]).astype(BF16)

    for s in range(NX):
        gated(s)
    reads(0)

    @pl.when(z < last)
    def _():
        remote(rim_out, rim_in, rim_sem.at[0], rim_sem.at[1], sp=z + 1).start()

    for s in range(1, NX):
        reads(s)

    def second(zz, _):
        for rel, core in ((0, c), (1, other)):
            first, again = wout.at[core * NX + left, zz], wout.at[core * NX + right, zz]
            arrived(first, near_recv.at[0, rel, zz])
            remote(first.at[0], first.at[0], far_send.at[0, rel, zz], far_recv.at[0, rel, zz], fs=right).start()
            arrived(again, near_recv.at[1, rel, zz])
            remote(again.at[1], again.at[1], far_send.at[1, rel, zz], far_recv.at[1, rel, zz], fs=left).start()
        return 0

    lax.fori_loop(0, half, second, 0)

    @pl.when(z > 0)
    def _():
        arrived(rim_in, rim_sem.at[1])
        extended[:, 0:PAD, :] = rim_in[...].astype(F32)

    @pl.when(z == 0)
    def _():
        extended[:, 0:PAD, :] = jnp.zeros((NX, PAD, HEAD), F32)

    piece = 64
    taps = taps_ref[:, lanes(head)]
    for s in range(NX):
        for r in range(rows // piece):
            conv = jnp.zeros((piece, HEAD), F32)
            for tap in range(KSIZE):
                conv = conv + taps[tap : tap + 1] * extended[s, pl.ds(r * piece + tap + PAD - KSIZE + 1, piece), :]
            conv_out[s, pl.ds(r * piece, piece), :] = conv.astype(BF16)

    def give(i):
        @pl.when(i != z)
        def _():
            remote(states.at[i], state_in.at[seq_me], state_send.at[i], state_recv.at[seq_me], sp=i).start()

        @pl.when(i == z)
        def _():
            pltpu.make_async_copy(states.at[i], state_in.at[seq_me], state_recv.at[seq_me]).start()

    @pl.when(is_composer)
    def _():
        arrived(start, s_recv.at[0])

        def advance(i, state):
            states[i] = state.astype(BF16)
            arrived(map_in.at[i], map_recv.at[i])
            block = map_in[i]
            keep = block[HEAD : HEAD + 1, :HEAD].astype(F32) + block[HEAD + 8 : HEAD + 9, :HEAD].astype(F32)
            high = state.astype(BF16)
            low = state - high.astype(F32)
            reduce = dot(block[:HEAD, HEAD:], high) + dot(block[:HEAD, HEAD:], low)
            result = keep * state - reduce + block[:HEAD, :HEAD].astype(F32)
            give(i)
            return result

        states[last] = lax.fori_loop(0, last, advance, start[...]).astype(BF16)

    def exchange(src, dst, send, recv):
        for d in range(NX):
            s = turn(x + d, NX)
            if d == 0:
                pltpu.make_async_copy(src.at[s], dst.at[:, lanes(head)], recv.at[0]).start()
            else:
                remote(src.at[s], dst.at[:, lanes(head)], send.at[d], recv.at[d], fs=s).start()
            remote(src.at[s], dst.at[:, lanes(head)], send.at[NX + d], recv.at[NX + d], fs=s, tp=other).start()

    def exchanged(src, dst, send, recv):
        for d in range(NX):
            source = turn(x - d, NX)
            arrived(dst.at[:, lanes(c * NX + source)], recv.at[d])
            arrived(dst.at[:, lanes(other * NX + source)], recv.at[NX + d])
            if d:
                remote(src.at[0], dst.at[:, lanes(head)], send.at[d], recv.at[d], fs=right).wait_send()
            remote(src.at[0], dst.at[:, lanes(head)], send.at[NX + d], recv.at[NX + d], fs=right).wait_send()

    exchange(conv_out, conv_all, conv_send, conv_recv)
    pl.when(is_composer)(lambda: give(last))

    head_gain = head_gain_ref[...]
    for s in range(NX):
        arrived(state_in.at[s], state_recv.at[s])
        attn = base[s] + jnp.dot(reader[s], state_in[s], preferred_element_type=F32)
        scale = lax.rsqrt(jnp.mean(attn * attn, axis=-1, keepdims=True) + EPS)
        attn_out[s] = (attn * scale * head_gain).astype(BF16)

    exchange(attn_out, attn_all, attn_send, attn_recv)
    exchanged(conv_out, conv_all, conv_send, conv_recv)

    def channel_norm(i, _):
        at = pl.ds(pl.multiple_of(i * 64, 64), 64)
        conv = conv_all[at, :].astype(F32)
        mean = jnp.mean(conv, axis=-1, keepdims=True)
        var = jnp.mean(conv * conv, axis=-1, keepdims=True) - mean * mean
        conv_all[at, :] = silu((conv - mean) * lax.rsqrt(var + EPS) * channel_gain_ref[...]).astype(BF16)
        return 0

    lax.fori_loop(0, rows // 64, channel_norm, 0)

    def weights_in(zz, _):
        arrived(wout.at[head, zz], own_recv.at[0, zz])
        arrived(wout.at[other * NX + x, zz], own_recv.at[1, zz])
        for rel, core in ((0, c), (1, other)):
            for kind in range(2):
                arrived(wout.at[core * NX + over, zz, kind], far_recv.at[kind, rel, zz])
        return 0

    lax.fori_loop(0, half, weights_in, 0)

    def weights(j, kind):
        return wout[:, j, kind].reshape(HEADS * HEAD, HEAD)

    def conv_part(j, _):
        partial[j] = jnp.dot(conv_all[...], weights(j, 1), preferred_element_type=F32)
        return 0

    lax.fori_loop(0, half, conv_part, 0)
    exchanged(attn_out, attn_all, attn_send, attn_recv)

    def attn_part(j, _):
        total = partial[j] + jnp.dot(attn_all[...], weights(j, 0), preferred_element_type=F32)
        out_ref[:, lanes(j)] = total.astype(BF16)
        return 0

    lax.fori_loop(0, half, attn_part, 0)

    for pos in range(count):
        for way in range(2):
            if half > 1:
                hop(half - 2, pos, way, z).wait_send()
            if pos % 2 == way:
                hop(half - 1, pos, way, z).wait_send()
    for i in range(2):
        for where, line in ((right, 0), (left, 1), (right, 2)):
            ref = tok.at[x, c, halves[i]]
            remote(ref, ref, t_send.at[line, i], t_recv.at[line, i], fs=where).wait_send()
    for i in range(4):
        remote(tok.at[x, c], tok.at[x, c], c_send.at[i], c_recv.at[i], tp=other).wait_send()
    for copy in spike_copies:
        copy.wait_send()

    @pl.when(is_composer & (x == seq_me))
    def _():
        for copy in start_sends:
            copy.wait_send()

    def drain(i, _):
        for way in range(2):
            remote(wring.at[i], wout.at[head, 0], near_send.at[way, i], near_recv.at[way, 0, 0], fs=right).wait_send()
        if paired:

            @pl.when(i != z)
            def _():
                a = block_of(i, 3)
                remote(a, a, y_send.at[i, 0], y_recv.at[i, 0], grp=partner).wait_send()
                b = wring.at[i, 0]
                remote(b, b, y_send.at[i, 1], y_recv.at[i, 1], grp=partner).wait_send()

        @pl.when(is_composer & (i != z))
        def _():
            remote(states.at[i], state_in.at[seq_me], state_send.at[i], state_recv.at[seq_me], sp=i).wait_send()

        return 0

    lax.fori_loop(0, nz, drain, 0)

    def drain_half(zz, _):
        remote(wring.at[0], wout.at[head, zz], own_send.at[zz], own_recv.at[1, zz], tp=other).wait_send()
        for way in range(2):
            for rel in range(2):
                ref = wout.at[head, zz, 0]
                remote(ref, ref, far_send.at[way, rel, zz], far_recv.at[way, rel, zz], fs=right).wait_send()
        return 0

    lax.fori_loop(0, half, drain_half, 0)
    for s in range(NX):

        @pl.when((z != s * quarter + quarter // 2) & (z != last))
        def _(s=s):
            remote(map_out.at[s], map_in.at[z], map_send.at[s], map_recv.at[z], sp=0).wait_send()

    @pl.when(z < last)
    def _():
        remote(rim_out, rim_in, rim_sem.at[0], rim_sem.at[1], sp=z + 1).wait_send()


def mixed_tokens(nz, paired, tokens, *rest):
    rows, features = tokens.shape
    half = nz // 2
    count = 5 if paired else 7
    vmem = pl.BlockSpec(memory_space=pltpu.VMEM)
    smem = pl.BlockSpec(memory_space=pltpu.SMEM)
    dma = pltpu.SemaphoreType.DMA
    width = HEADS * HEAD
    return pl.pallas_call(
        functools.partial(kernel, nz, paired),
        name="mix",
        out_shape=jax.ShapeDtypeStruct((rows, half * HEAD), BF16),
        in_specs=[vmem] * 13 + [smem] * 2 + [vmem] * 3,
        out_specs=vmem,
        scratch_shapes=[
            pltpu.VMEM((NX, 2, rows, features), BF16),
            pltpu.VMEM((NX * rows, 2 * features), BF16),
            pltpu.VMEM((nz * HEAD, 5 * HEAD), BF16),
            pltpu.VMEM((nz, 2, HEAD, HEAD), BF16),
            pltpu.VMEM((HEADS, half, 2, HEAD, HEAD), BF16),
            pltpu.VMEM((8, rows), F32),
            pltpu.VMEM((NX, 8, rows), F32),
            pltpu.VMEM((HEAD, HEAD), F32),
            pltpu.VMEM((NX, rows, HEAD), BF16),
            pltpu.VMEM((NX, rows, rows), F32),
            pltpu.VMEM((NX, rows, HEAD), F32),
            pltpu.VMEM((NX, rows, 2 * HEAD), BF16),
            pltpu.VMEM((NX, rows, HEAD), F32),
            pltpu.VMEM((NX, rows, HEAD), BF16),
            pltpu.VMEM((NX, HEAD + 16, 2 * HEAD), BF16),
            pltpu.VMEM((nz, HEAD + 16, 2 * HEAD), BF16),
            pltpu.VMEM((nz, HEAD, HEAD), BF16),
            pltpu.VMEM((NX, HEAD, HEAD), BF16),
            pltpu.VMEM((NX, PAD, HEAD), BF16),
            pltpu.VMEM((NX, PAD, HEAD), BF16),
            pltpu.VMEM((NX, PAD + rows, HEAD), F32),
            pltpu.VMEM((NX, rows, HEAD), BF16),
            pltpu.VMEM((rows, width), BF16),
            pltpu.VMEM((NX, rows, HEAD), BF16),
            pltpu.VMEM((rows, width), BF16),
            pltpu.VMEM((half, rows, HEAD), F32),
            dma((2, 2, count)),
            dma((2, half, count)),
            dma((nz, 2)),
            dma((nz, 2)),
            dma((2, nz)),
            dma((2, 2, half)),
            dma((2, 2, half)),
            dma((2, 2, half)),
            dma((half,)),
            dma((2, half)),
            dma((3, 2)),
            dma((3, 2)),
            dma((4,)),
            dma((4,)),
            dma((3,)),
            dma((3,)),
            dma((3,)),
            dma((1,)),
            dma((9,)),
            dma((NX,)),
            dma((nz,)),
            dma((nz,)),
            dma((NX,)),
            dma((2,)),
            dma((2 * NX,)),
            dma((2 * NX,)),
            dma((2 * NX,)),
            dma((2 * NX,)),
        ],
        compiler_params=pltpu.CompilerParams(
            collective_id=0, has_side_effects=True, vmem_limit_bytes=60 * 1024 * 1024
        ),
    )(tokens, *rest)


def on_device(
    nz,
    paired,
    tokens,
    input_norm_gain,
    query_weight,
    key_weight,
    value_weight,
    decay_gate_weight,
    write_strength_weight,
    up_weight,
    gate_half_weight,
    log_decay_rate,
    write_strength_bias,
    decay_spike_added,
    starting_state,
    head_norm_gain,
    convolution_kernel,
    channel_norm_gain,
    delta_output_rows,
    convolution_output_rows,
):
    mixed = mixed_tokens(
        nz,
        paired,
        tokens[0],
        key_weight,
        value_weight,
        query_weight,
        up_weight,
        gate_half_weight,
        delta_output_rows,
        convolution_output_rows,
        input_norm_gain[None],
        decay_gate_weight,
        write_strength_weight,
        decay_spike_added[0],
        starting_state[0],
        log_decay_rate,
        write_strength_bias,
        head_norm_gain[None],
        convolution_kernel,
        channel_norm_gain[None],
    )
    return mixed[None]


def solution(mesh):
    return jax.shard_map(
        functools.partial(on_device, mesh.shape["sp"], mesh.shape["grp"] % 2 == 0),
        mesh=mesh,
        in_specs=(
            P(("grp", "fs"), "sp", "tp"),
            P(),
            P("sp", "tp"),
            P("sp", "tp"),
            P("sp", "tp"),
            P(),
            P(),
            P("sp", "tp"),
            P("sp", "tp"),
            P(),
            P(),
            P(("grp", "fs"), "sp", "tp"),
            P(("grp", "fs"), "tp", None, None),
            P(),
            P(),
            P(),
            P("tp", "sp"),
            P("tp", "sp"),
        ),
        out_specs=P(("grp", "fs"), "sp", "tp"),
        check_vma=False,
    )
```

time: 147 us -> 119 us (0.81)
  Pallas kernels: 141 us -> 113 us
    pallas_call x2 -> x1, Pallas kernels: 141 us -> 113 us  [mixed_tokens(): pl.pallas_call(functools.partial(kernel, nz, paired), name='mix', out_sha...]
    unnamed x1 -> x10, local copies, waits for them, and re-layouts: 1.87 us -> 5.36 us
    pad x2 -> x0, local copies, waits for them, and re-layouts: 2.18 us -> none  [the longest x1 1.28 us: on_device(): spike = jnp.pad(decay_spike_added[0].T, ((0, 8 - NX), (0, 0)))]
where the time goes in v2:
time: 119 us
  Pallas kernels  113 us (95%)
  local copies, waits for them, and re-layouts  5.36 us (5%)
    pallas_call x1, Pallas kernels, mixed_tokens(): pl.pallas_call(functools.partial(kernel, nz, paired), name='mix', out_sha...  113 us
    unnamed x10, local copies, waits for them, and re-layouts  5.36 us

profile of v2, /device:TPU:33, one launch (start us, length us, event | category | flops | bytes accessed | tf_op | source)
XLA Modules:
  0.0 118.6 jit_solution(6769916506390340573)
XLA Ops:
  0.0 0.0 copy-start.2
  0.0 0.7 copy-done.2
  0.7 0.0 copy-start
  0.7 0.8 copy.19
  1.5 0.0 copy-done
  1.5 0.0 copy-start.1
  1.5 1.0 copy.20.decay_ref
  2.5 0.0 copy-done.1
  2.5 1.0 copy.21.strength_ref
  3.5 113.2 %mix.1 = bf16[256,1024]{1,0:T(8,128)(2,1)} custom-call(bf16[256,1024]{1,0:T(8,128)(2,1)} %bitcast.9, bf16[128,512]{1,0:T(8,128)(2,1)} %k_ref.1, bf16[128,512]{1,0:T(8,128)(2,1)} %v_ref.1, bf16[128,512]{1,0:T(8,128)(2,1)} %q_ref.1, bf16[128,512]{1,0:T(8,128)(2,1)} %up_ref.1, bf16[128,512]{1,0:T(8,128)(2,1)} %gate_ref.1, bf16[512,128]{1,0:T(8,128)(2,1)} %do_ref.1, ...), custom_call_target="tpu_custom_call" | custom-call | tf_op jit(solution)/shard_map/mix/pallas_call | solution.py:651
  116.7 1.9 %copy.23 = bf16[1,256,1024]{2,1,0:T(8,128)(2,1)} copy(bf16[1,256,1024]{2,1,0:T(8,128)(2,1)} %bitcast.7) | data formatting | bytes 1048576
Async XLA Ops:
  0.0 0.7 copy-start.2
  0.7 0.8 copy-start
  1.5 1.0 copy-start.1

commit v3 on v2

--- a/solution.py
+++ b/solution.py
@@ -63,17 +63,19 @@
     return a * lax.rsqrt(jnp.sum(a * a, axis=-1, keepdims=True) + EPS)
 
 
-def unit_lower_inverse(a, row, col):
-    size = a.shape[0]
+def unit_lower_inverses(blocks, row, col):
+    size = blocks[0].shape[0]
     eye = jnp.where(row == col, 1.0, 0.0)
-    inverse = eye - jnp.where((row - col == 1) & (lax.rem(row, 2) == 1), a, 0.0)
+    below = (row - col == 1) & (lax.rem(row, 2) == 1)
+    inverses = [eye - jnp.where(below, a, 0.0) for a in blocks]
     width = 2
     while width < size:
         same = lax.div(row, 2 * width) == lax.div(col, 2 * width)
-        block = jnp.where(same & (lax.div(row, width) != lax.div(col, width)), a, 0.0)
-        inverse = inverse - dot(dot(inverse, block), inverse)
+        mask = same & (lax.div(row, width) != lax.div(col, width))
+        steps = [dot(b, jnp.where(mask, a, 0.0)) for a, b in zip(blocks, inverses)]
+        inverses = [b - dot(p, b) for p, b in zip(steps, inverses)]
         width *= 2
-    return inverse
+    return inverses
 
 
 def kernel(
@@ -100,10 +102,9 @@
     out_ref,
     tok,
     normed,
-    win,
-    wring,
+    wbuf,
     wout,
-    spike_rows,
+    gates,
     spikes,
     start,
     keys_at,
@@ -175,13 +176,9 @@
     for where in neighbours:
         pl.semaphore_signal(barrier, inc=1, device_id=where, device_id_type=MESH)
 
-    def block_of(src, j):
-        return win.at[pl.ds(pl.multiple_of(src * HEAD, HEAD), HEAD), lanes(j)]
-
     own = [w.at[:, lanes(x)] for w in (k_ref, v_ref, q_ref, up_ref, gate_ref)]
     own += [w.at[lanes(x), :] for w in (do_ref, co_ref)]
-    own_at = [block_of(z, j) for j in range(5)] + [wring.at[z, j] for j in range(2)]
-    copies = [pltpu.make_async_copy(a, b, local.at[j]) for j, (a, b) in enumerate(zip(own, own_at))]
+    copies = [pltpu.make_async_copy(a, wbuf.at[z, j], local.at[j]) for j, a in enumerate(own)]
     copies.append(pltpu.make_async_copy(tok_ref, tok.at[x, c], local.at[7]))
     for copy in copies:
         copy.start()
@@ -195,30 +192,28 @@
     def to_column(line):
         return jnp.sum(jnp.where(row == col, line, 0.0), axis=1, keepdims=True)
 
-    spike = spike_ref[...]
-    spike_rows[...] = jnp.zeros_like(spike_rows)
-    for i in range(NX):
-        spike_rows[i : i + 1, :] = to_row(spike[:, i : i + 1])
-
     if paired:
-        places = [lambda src, j=j: block_of(src, j) for j in range(3)]
-        places += [lambda src: block_of(src, 3 + parity), lambda src: wring.at[src, parity]]
-        shared = {3: 0, 4: 1}
+        chunks, shared = [0, 1, 2, 3 + parity, 5 + parity], (3, 4)
     else:
-        places = [lambda src, j=j: block_of(src, j) for j in range(5)]
-        places += [lambda src, j=j: wring.at[src, j] for j in range(2)]
-        shared = {}
-    count = len(places)
+        chunks, shared = list(range(7)), ()
+    count = len(chunks)
 
     def hop(t, pos, way, src):
-        ref = places[pos](src)
-        sem = ring_send.at[way, lax.rem(t, 2), pos]
-        return remote(ref, ref, sem, ring_recv.at[way, t, pos], sp=up if way == 0 else down)
+        ref = wbuf.at[src, chunks[pos]]
+        return remote(ref, ref, ring_send.at[way, t, pos], ring_recv.at[way, t, pos], sp=up if way == 0 else down)
+
+    def to_partner(src, i):
+        ref = wbuf.at[src, chunks[shared[i]]]
+        return remote(ref, ref, y_send.at[src, i], y_recv.at[src, i], grp=partner)
+
+    def whole_piece(src):
+        if paired:
+            arrived(wbuf.at[src, 6 - parity], y_recv.at[src, 1])
 
     def spread(src):
         core, zz = lax.div(src, half), lax.rem(src, half)
         other_core = core + c - 2 * core * c
-        piece, target = wring.at[src], wout.at[head, zz]
+        piece, target = wbuf.at[src, pl.ds(5, 2)], wout.at[head, zz]
         remote(piece, target, near_send.at[0, src], near_recv.at[0, other_core, zz], fs=right, tp=core).start()
         remote(piece, target, near_send.at[1, src], near_recv.at[1, other_core, zz], fs=left, tp=core).start()
 
@@ -246,11 +241,11 @@
         remote(src, dst, t_send.at[1, i], t_recv.at[1, i], fs=left).start()
     remote(tok_ref, tok.at[x, c], c_send.at[0], c_recv.at[0], tp=other).start()
     spike_copies = [
-        remote(spike_rows, spikes.at[x], k_send.at[d - 1], k_recv.at[d - 1], fs=turn(x + d, NX)) for d in (1, 2, 3)
+        remote(spike_ref, spikes.at[x], k_send.at[d - 1], k_recv.at[d - 1], fs=turn(x + d, NX)) for d in (1, 2, 3)
     ]
     for copy in spike_copies:
         copy.start()
-    spike_own = pltpu.make_async_copy(spike_rows, spikes.at[x], local.at[8])
+    spike_own = pltpu.make_async_copy(spike_ref, spikes.at[x], local.at[8])
     spike_own.start()
 
     start_sends = [
@@ -316,88 +311,93 @@
         (6, tokens_far),
     )
 
-    def ring(t, _):
-        back, fore = turn(z - t, nz), turn(z + t, nz)
+    for t in range(1, half):
+        both_ways = ((0, turn(z - t, nz)), (1, turn(z + t, nz)))
         for pos in range(count):
-            for way, src in ((0, back), (1, fore)):
-                arrived(places[pos](src), ring_recv.at[way, t - 1, pos])
-
-                @pl.when(t >= 2)
-                def _(pos=pos, way=way):
-                    hop(t, pos, way, z).wait_send()
-
-                @pl.when((t < half - 1) | (pos % 2 == way))
-                def _(pos=pos, way=way, src=src):
+            for way, src in both_ways:
+                arrived(wbuf.at[src, chunks[pos]], ring_recv.at[way, t - 1, pos])
+                if t < half - 1 or pos % 2 == way:
                     hop(t, pos, way, src).start()
-
-                if pos in shared:
-                    ref = places[pos](src)
-                    i = shared[pos]
-                    remote(ref, ref, y_send.at[src, i], y_recv.at[src, i], grp=partner).start()
-
-        @pl.when(t >= 2)
-        def _():
+        for i in range(len(shared)):
+            for way, src in both_ways:
+                to_partner(src, i).start()
+        if t >= 2:
             for src in (turn(z - t + 1, nz), turn(z + t - 1, nz)):
-                if paired:
-                    arrived(wring.at[src, 1 - parity], y_recv.at[src, 1])
+                whole_piece(src)
                 spread(src)
-
         for when, task in hooks:
-            pl.when(t == min(when, half - 1))(task)
-        return 0
-
-    lax.fori_loop(1, half, ring, 0)
+            if t == min(when, half - 1):
+                task()
     far = turn(z + half, nz)
     for pos in range(count):
-        arrived(places[pos](far), ring_recv.at[pos % 2, half - 1, pos])
-        if pos in shared:
-            ref = places[pos](far)
-            i = shared[pos]
-            remote(ref, ref, y_send.at[far, i], y_recv.at[far, i], grp=partner).start()
+        arrived(wbuf.at[far, chunks[pos]], ring_recv.at[pos % 2, half - 1, pos])
+    for i in range(len(shared)):
+        to_partner(far, i).start()
     norm_near(3, over)
+    for src in (turn(z - half + 1, nz), turn(z + half - 1, nz)):
+        whole_piece(src)
+        spread(src)
 
     for d in (1, 2, 3):
         arrived(spikes.at[turn(x - d, NX)], k_recv.at[d - 1])
     spike_own.wait()
 
-    rate = jnp.exp(jnp.full((rows, 1), rate_ref[head], F32))
+    def matrix(*js):
+        return jnp.concatenate([wbuf[:, j].reshape(nz * HEAD, HEAD) for j in js], axis=1)
+
+    def rows_of(s):
+        return pl.ds(pl.multiple_of(s * rows, rows), rows)
+
+    small = jnp.concatenate([decay_ref[...], strength_ref[...]], axis=0)
+    for s in range(NX):
+        gates[s] = dot_t(small, normed[s * rows : (s + 1) * rows, :])
+    rate = jnp.exp(jnp.full((1, rows), rate_ref[head], F32))
     bias = bias_ref[head]
-    lane = lax.broadcasted_iota(jnp.int32, (rows, HEADS), 1)
-
-    def delta(s):
-        at = pl.ds(s * rows, rows)
-        tokens = normed[at, :]
-        raw = jnp.dot(tokens, win[:, : 2 * HEAD], preferred_element_type=F32).astype(BF16).astype(F32)
+    edge = rows // 2
+    row_half = lax.broadcasted_iota(jnp.int32, (edge, edge), 0)
+    col_half = lax.broadcasted_iota(jnp.int32, (edge, edge), 1)
+
+    def rounded(a):
+        return a.astype(BF16).astype(F32)
+
+    def terms(s):
+        raw = rounded(jnp.dot(normed[rows_of(s), :], matrix(0, 1), preferred_element_type=F32))
         keys = unit_rows(silu(raw[:, :HEAD]))
         values = silu(raw[:, HEAD:])
-
-        def gate(ref):
-            both = jnp.dot(tokens, ref[...], preferred_element_type=F32).astype(BF16).astype(F32)
-            return jnp.sum(jnp.where(lane == head, both, 0.0), axis=1, keepdims=True)
-
-        logit = gate(decay_ref)
-        beta = jax.nn.sigmoid(gate(strength_ref) + bias)
+        logit = rounded(gates[s, pl.ds(head, 1), :])
+        beta = to_column(jax.nn.sigmoid(rounded(gates[s, pl.ds(HEADS + head, 1), :]) + bias))
         soft = jnp.maximum(logit, 0.0) + jnp.log1p(jnp.exp(-jnp.abs(logit)))
-        log_col = to_column(spikes[s, pl.ds(x, 1), :]) - rate * soft
-        log_row = to_row(log_col)
+        log_row = spikes[s, pl.ds(x, 1), :] - rate * soft
         cum_col = jnp.sum(jnp.where(col <= row, log_row, 0.0), axis=1, keepdims=True)
-        cum_row = jnp.sum(jnp.where(row <= col, log_col, 0.0), axis=0, keepdims=True)
-        total = cum_col[rows - 1 :, :]
+        cum_row = to_row(cum_col)
         gamma = jnp.where(col <= row, jnp.exp(jnp.minimum(cum_col - cum_row, 0.0)), 0.0)
         grown = jnp.exp(cum_col)
         a_matrix = jnp.where(col < row, beta * dot_t(keys, keys) * gamma, 0.0)
-        inverse = unit_lower_inverse(a_matrix, row, col)
-        both = dot(inverse, jnp.concatenate([beta * values, (beta * grown) * keys], axis=1)).astype(BF16)
-        mapped = dot_of_t(keys * jnp.exp(total - cum_col), both)
-        keep = jnp.exp(total)
-        keep_hi = keep.astype(BF16).astype(F32)
-        tail = lax.broadcasted_iota(jnp.int32, (16, 2 * HEAD), 0)
-        map_out[s, 0:HEAD, :] = mapped.astype(BF16)
-        map_out[s, HEAD:, :] = jnp.where(tail < 8, keep_hi, keep - keep_hi).astype(BF16)
+        right = jnp.concatenate([beta * values, (beta * grown) * keys], axis=1).astype(BF16)
+        total = cum_col[rows - 1 :, :]
+        decayed = (keys * jnp.exp(total - cum_col)).astype(BF16)
         keys_at[s] = keys.astype(BF16)
         gammas[s] = gamma
         growth[s] = jnp.broadcast_to(grown, (rows, HEAD))
-        solved[s] = both
+        return a_matrix, right, decayed, total
+
+    def finish(group_of, all_terms):
+        blocks = []
+        for a_matrix, _, _, _ in all_terms:
+            blocks += [a_matrix[:edge, :edge], a_matrix[edge:, edge:]]
+        inverses = unit_lower_inverses(blocks, row_half, col_half)
+        for n, s in enumerate(group_of):
+            a_matrix, right, decayed, total = all_terms[n]
+            first, second_half = inverses[2 * n], inverses[2 * n + 1]
+            top = dot(first, right[:edge])
+            low = dot(second_half, right[edge:].astype(F32) - dot(a_matrix[edge:, :edge], top))
+            both = jnp.concatenate([top, low], axis=0).astype(BF16)
+            solved[s] = both
+            keep = jnp.exp(total)
+            keep_hi = rounded(keep)
+            tail = lax.broadcasted_iota(jnp.int32, (16, 2 * HEAD), 0)
+            map_out[s, 0:HEAD, :] = dot_of_t(decayed, both).astype(BF16)
+            map_out[s, HEAD:, :] = jnp.where(tail < 8, keep_hi, keep - keep_hi).astype(BF16)
 
     def send_map(s):
         owner = s * quarter + quarter // 2
@@ -410,51 +410,26 @@
         def _():
             pltpu.make_async_copy(map_out.at[s], map_in.at[z], map_recv.at[z]).start()
 
-    for s in range(NX):
-        delta(s)
-        if s:
-            send_map(s - 1)
-
-    for src in (turn(z - half + 1, nz), turn(z + half - 1, nz), far):
-        if paired:
-            arrived(wring.at[src, 1 - parity], y_recv.at[src, 1])
-        spread(src)
-    send_map(NX - 1)
+    here = lax.div(z, quarter)
+    far_pair = [lax.rem(here + k, NX) for k in (2, 1)]
+    near_pair = [lax.rem(here + k, NX) for k in (3, 0)]
+    finish(far_pair, [terms(s) for s in far_pair])
+    whole_piece(far)
+    spread(far)
+    pending = [terms(s) for s in near_pair]
+    for s in far_pair:
+        send_map(s)
+    finish(near_pair, pending)
     if paired:
 
         def shared_in(d, _):
             src = turn(z + d, nz)
-            arrived(block_of(src, 4 - parity), y_recv.at[src, 0])
+            arrived(wbuf.at[src, 4 - parity], y_recv.at[src, 0])
             return 0
 
         lax.fori_loop(1, nz, shared_in, 0)
-
-    def gated(s):
-        at = pl.ds(s * rows, rows)
-        raw = jnp.dot(normed[at, :], win[:, 3 * HEAD :], preferred_element_type=F32).astype(BF16).astype(F32)
-        glu = (raw[:, :HEAD] * jax.nn.sigmoid(raw[:, HEAD:])).astype(BF16)
-        extended[s, pl.ds(PAD, rows), :] = glu.astype(F32)
-        rim_out[s] = glu[rows - PAD :]
-
-    def reads(s):
-        at = pl.ds(s * rows, rows)
-        raw = jnp.dot(normed[at, :], win[:, 2 * HEAD : 3 * HEAD], preferred_element_type=F32).astype(BF16).astype(F32)
-        query = unit_rows(silu(raw)) * HEAD ** (-0.5)
-        scores = dot_t(query, keys_at[s]) * gammas[s]
-        read = dot(scores, solved[s])
-        base[s] = read[:, :HEAD]
-        reader[s] = (growth[s] * query - read[:, HEAD:]).astype(BF16)
-
-    for s in range(NX):
-        gated(s)
-    reads(0)
-
-    @pl.when(z < last)
-    def _():
-        remote(rim_out, rim_in, rim_sem.at[0], rim_sem.at[1], sp=z + 1).start()
-
-    for s in range(1, NX):
-        reads(s)
+    for s in near_pair:
+        send_map(s)
 
     def second(zz, _):
         for rel, core in ((0, c), (1, other)):
@@ -466,6 +441,33 @@
         return 0
 
     lax.fori_loop(0, half, second, 0)
+
+    def gated(s):
+        at = pl.ds(s * rows, rows)
+        raw = rounded(jnp.dot(normed[at, :], matrix(3, 4), preferred_element_type=F32))
+        glu = (raw[:, :HEAD] * jax.nn.sigmoid(raw[:, HEAD:])).astype(BF16)
+        extended[s, pl.ds(PAD, rows), :] = glu.astype(F32)
+        rim_out[s] = glu[rows - PAD :]
+
+    def reads(s):
+        at = pl.ds(s * rows, rows)
+        raw = rounded(jnp.dot(normed[at, :], matrix(2), preferred_element_type=F32))
+        query = unit_rows(silu(raw)) * HEAD ** (-0.5)
+        scores = dot_t(query, keys_at[s]) * gammas[s]
+        read = dot(scores, solved[s])
+        base[s] = read[:, :HEAD]
+        reader[s] = (growth[s] * query - read[:, HEAD:]).astype(BF16)
+
+    for s in range(NX):
+        gated(s)
+    reads(0)
+
+    @pl.when(z < last)
+    def _():
+        remote(rim_out, rim_in, rim_sem.at[0], rim_sem.at[1], sp=z + 1).start()
+
+    for s in range(1, NX):
+        reads(s)
 
     @pl.when(z > 0)
     def _():
@@ -534,13 +536,30 @@
     pl.when(is_composer)(lambda: give(last))
 
     head_gain = head_gain_ref[...]
-    for s in range(NX):
+    target = attn_all.at[:, lanes(head)]
+
+    def send_attn(s):
+        d = turn(s - x, NX)
+
+        @pl.when(d == 0)
+        def _():
+            pltpu.make_async_copy(attn_out.at[s], target, attn_recv.at[0]).start()
+
+        @pl.when(d != 0)
+        def _():
+            remote(attn_out.at[s], target, attn_send.at[d], attn_recv.at[d], fs=s).start()
+
+        remote(attn_out.at[s], target, attn_send.at[NX + d], attn_recv.at[NX + d], fs=s, tp=other).start()
+
+    order = [lax.rem(here + k, NX) for k in (0, 1, 3, 2)]
+    for n, s in enumerate(order):
         arrived(state_in.at[s], state_recv.at[s])
         attn = base[s] + jnp.dot(reader[s], state_in[s], preferred_element_type=F32)
         scale = lax.rsqrt(jnp.mean(attn * attn, axis=-1, keepdims=True) + EPS)
         attn_out[s] = (attn * scale * head_gain).astype(BF16)
-
-    exchange(attn_out, attn_all, attn_send, attn_recv)
+        if n:
+            send_attn(order[n - 1])
+    send_attn(order[-1])
     exchanged(conv_out, conv_all, conv_send, conv_recv)
 
     def channel_norm(i, _):
@@ -564,28 +583,32 @@
     lax.fori_loop(0, half, weights_in, 0)
 
     def weights(j, kind):
-        return wout[:, j, kind].reshape(HEADS * HEAD, HEAD)
+        pair = [wout[:, 2 * j + i, kind].reshape(HEADS * HEAD, HEAD) for i in range(2)]
+        return jnp.concatenate(pair, axis=1)
 
     def conv_part(j, _):
         partial[j] = jnp.dot(conv_all[...], weights(j, 1), preferred_element_type=F32)
         return 0
 
-    lax.fori_loop(0, half, conv_part, 0)
+    lax.fori_loop(0, half // 2, conv_part, 0)
     exchanged(attn_out, attn_all, attn_send, attn_recv)
 
     def attn_part(j, _):
         total = partial[j] + jnp.dot(attn_all[...], weights(j, 0), preferred_element_type=F32)
-        out_ref[:, lanes(j)] = total.astype(BF16)
+        out_ref[:, pl.ds(pl.multiple_of(j * 2 * HEAD, 2 * HEAD), 2 * HEAD)] = total.astype(BF16)
         return 0
 
-    lax.fori_loop(0, half, attn_part, 0)
-
+    lax.fori_loop(0, half // 2, attn_part, 0)
+
+    def drain_ring(t, _):
+        for pos in range(count):
+            for way in range(2):
+                hop(t, pos, way, z).wait_send()
+        return 0
+
+    lax.fori_loop(0, half - 1, drain_ring, 0)
     for pos in range(count):
-        for way in range(2):
-            if half > 1:
-                hop(half - 2, pos, way, z).wait_send()
-            if pos % 2 == way:
-                hop(half - 1, pos, way, z).wait_send()
+        hop(half - 1, pos, pos % 2, z).wait_send()
     for i in range(2):
         for where, line in ((right, 0), (left, 1), (right, 2)):
             ref = tok.at[x, c, halves[i]]
@@ -602,15 +625,13 @@
 
     def drain(i, _):
         for way in range(2):
-            remote(wring.at[i], wout.at[head, 0], near_send.at[way, i], near_recv.at[way, 0, 0], fs=right).wait_send()
+            remote(wbuf.at[i, pl.ds(5, 2)], wout.at[head, 0], near_send.at[way, i], near_recv.at[way, 0, 0], fs=right).wait_send()
         if paired:
 
             @pl.when(i != z)
             def _():
-                a = block_of(i, 3)
-                remote(a, a, y_send.at[i, 0], y_recv.at[i, 0], grp=partner).wait_send()
-                b = wring.at[i, 0]
-                remote(b, b, y_send.at[i, 1], y_recv.at[i, 1], grp=partner).wait_send()
+                to_partner(i, 0).wait_send()
+                to_partner(i, 1).wait_send()
 
         @pl.when(is_composer & (i != z))
         def _():
@@ -621,7 +642,7 @@
     lax.fori_loop(0, nz, drain, 0)
 
     def drain_half(zz, _):
-        remote(wring.at[0], wout.at[head, zz], own_send.at[zz], own_recv.at[1, zz], tp=other).wait_send()
+        remote(wbuf.at[0, pl.ds(5, 2)], wout.at[head, zz], own_send.at[zz], own_recv.at[1, zz], tp=other).wait_send()
         for way in range(2):
             for rel in range(2):
                 ref = wout.at[head, zz, 0]
@@ -657,11 +678,10 @@
         scratch_shapes=[
             pltpu.VMEM((NX, 2, rows, features), BF16),
             pltpu.VMEM((NX * rows, 2 * features), BF16),
-            pltpu.VMEM((nz * HEAD, 5 * HEAD), BF16),
-            pltpu.VMEM((nz, 2, HEAD, HEAD), BF16),
+            pltpu.VMEM((nz, 7, HEAD, HEAD), BF16),
             pltpu.VMEM((HEADS, half, 2, HEAD, HEAD), BF16),
-            pltpu.VMEM((8, rows), F32),
-            pltpu.VMEM((NX, 8, rows), F32),
+            pltpu.VMEM((NX, 2 * HEADS, rows), F32),
+            pltpu.VMEM((NX, NX, rows), F32),
             pltpu.VMEM((HEAD, HEAD), F32),
             pltpu.VMEM((NX, rows, HEAD), BF16),
             pltpu.VMEM((NX, rows, rows), F32),
@@ -680,8 +700,8 @@
             pltpu.VMEM((rows, width), BF16),
             pltpu.VMEM((NX, rows, HEAD), BF16),
             pltpu.VMEM((rows, width), BF16),
-            pltpu.VMEM((half, rows, HEAD), F32),
-            dma((2, 2, count)),
+            pltpu.VMEM((half // 2, rows, 2 * HEAD), F32),
+            dma((2, half, count)),
             dma((2, half, count)),
             dma((nz, 2)),
             dma((nz, 2)),
@@ -750,9 +770,9 @@
         delta_output_rows,
         convolution_output_rows,
         input_norm_gain[None],
-        decay_gate_weight,
-        write_strength_weight,
-        decay_spike_added[0],
+        decay_gate_weight.T,
+        write_strength_weight.T,
+        decay_spike_added[0].T,
         starting_state[0],
         log_decay_rate,
         write_strength_bias,

time: 119 us -> 110 us (0.924)
  Pallas kernels: 113 us -> 108 us
  local copies, waits for them, and re-layouts: 5.36 us -> 1.87 us
    pallas_call x1, Pallas kernels: 113 us -> 108 us  [mixed_tokens(): pl.pallas_call(functools.partial(kernel, nz, paired), name='mix', out_sha...]
    unnamed x10 -> x1, local copies, waits for them, and re-layouts: 5.36 us -> 1.87 us
where the time goes in v3:
time: 110 us
  Pallas kernels  108 us (98%)
  local copies, waits for them, and re-layouts  1.87 us (2%)
    pallas_call x1, Pallas kernels, mixed_tokens(): pl.pallas_call(functools.partial(kernel, nz, paired), name='mix', out_sha...  108 us

profile of v3, /device:TPU:33, one launch (start us, length us, event | category | flops | bytes accessed | tf_op | source)
XLA Modules:
  0.0 109.7 jit_solution(5457597527616243228)
XLA Ops:
  0.0 107.8 %mix.1 = bf16[256,1024]{1,0:T(8,128)(2,1)} custom-call(bf16[256,1024]{1,0:T(8,128)(2,1)} %bitcast.12, bf16[128,512]{1,0:T(8,128)(2,1)} %k_ref.1, bf16[128,512]{1,0:T(8,128)(2,1)} %v_ref.1, bf16[128,512]{1,0:T(8,128)(2,1)} %q_ref.1, bf16[128,512]{1,0:T(8,128)(2,1)} %up_ref.1, bf16[128,512]{1,0:T(8,128)(2,1)} %gate_ref.1, bf16[512,128]{1,0:T(8,128)(2,1)} %do_ref.1, ...), custom_call_target="tpu_custom_call" | custom-call | tf_op jit(solution)/shard_map/mix/pallas_call | solution.py:672
  107.8 1.9 %copy.20 = bf16[1,256,1024]{2,1,0:T(8,128)(2,1)} copy(bf16[1,256,1024]{2,1,0:T(8,128)(2,1)} %bitcast.11) | data formatting | bytes 1048576

commit v4 on v3

--- a/solution.py
+++ b/solution.py
@@ -36,9 +36,9 @@
     return pl.ds(pl.multiple_of(i * HEAD, HEAD), HEAD)
 
 
-def composer(z, nz):
+def composer(z, c, nz):
     quarter = nz // NX
-    return lax.div(z, quarter), lax.rem(z, quarter) == quarter // 2
+    return lax.div(z, quarter), lax.rem(z, quarter) == (1 - c) * (quarter // 2)
 
 
 def dot(a, b):
@@ -163,7 +163,7 @@
     quarter = nz // NX
     last = nz - 1
     rows, features = tok_ref.shape
-    seq_me, is_composer = composer(z, nz)
+    seq_me, is_composer = composer(z, c, nz)
     group = lax.axis_index("grp")
     parity = lax.rem(group, 2)
     partner = group + 1 - 2 * parity
@@ -328,15 +328,17 @@
         for when, task in hooks:
             if t == min(when, half - 1):
                 task()
-    far = turn(z + half, nz)
-    for pos in range(count):
-        arrived(wbuf.at[far, chunks[pos]], ring_recv.at[pos % 2, half - 1, pos])
-    for i in range(len(shared)):
-        to_partner(far, i).start()
     norm_near(3, over)
     for src in (turn(z - half + 1, nz), turn(z + half - 1, nz)):
         whole_piece(src)
         spread(src)
+    far = turn(z + half, nz)
+
+    def last_hop(positions):
+        for pos in positions:
+            arrived(wbuf.at[far, chunks[pos]], ring_recv.at[pos % 2, half - 1, pos])
+
+    last_hop(range(2))
 
     for d in (1, 2, 3):
         arrived(spikes.at[turn(x - d, NX)], k_recv.at[d - 1])
@@ -395,12 +397,12 @@
             solved[s] = both
             keep = jnp.exp(total)
             keep_hi = rounded(keep)
-            tail = lax.broadcasted_iota(jnp.int32, (16, 2 * HEAD), 0)
+            tail = lax.broadcasted_iota(jnp.int32, (8, 2 * HEAD), 0)
             map_out[s, 0:HEAD, :] = dot_of_t(decayed, both).astype(BF16)
-            map_out[s, HEAD:, :] = jnp.where(tail < 8, keep_hi, keep - keep_hi).astype(BF16)
+            map_out[s, HEAD:, :] = jnp.where(tail < 4, keep_hi, keep - keep_hi).astype(BF16)
 
     def send_map(s):
-        owner = s * quarter + quarter // 2
+        owner = s * quarter + other * (quarter // 2)
 
         @pl.when((z != owner) & (z != last))
         def _():
@@ -409,17 +411,32 @@
         @pl.when((z == owner) & (z != last))
         def _():
             pltpu.make_async_copy(map_out.at[s], map_in.at[z], map_recv.at[z]).start()
+
+    def reads(s):
+        at = rows_of(s)
+        raw = rounded(jnp.dot(normed[at, :], matrix(2), preferred_element_type=F32))
+        query = unit_rows(silu(raw)) * HEAD ** (-0.5)
+        scores = dot_t(query, keys_at[s]) * gammas[s]
+        read = dot(scores, solved[s])
+        base[s] = read[:, :HEAD]
+        reader[s] = (growth[s] * query - read[:, HEAD:]).astype(BF16)
 
     here = lax.div(z, quarter)
     far_pair = [lax.rem(here + k, NX) for k in (2, 1)]
     near_pair = [lax.rem(here + k, NX) for k in (3, 0)]
     finish(far_pair, [terms(s) for s in far_pair])
-    whole_piece(far)
-    spread(far)
+    last_hop(range(2, count))
+    for i in range(len(shared)):
+        to_partner(far, i).start()
     pending = [terms(s) for s in near_pair]
     for s in far_pair:
         send_map(s)
     finish(near_pair, pending)
+    reads(far_pair[0])
+    for s in near_pair:
+        send_map(s)
+    whole_piece(far)
+    spread(far)
     if paired:
 
         def shared_in(d, _):
@@ -428,8 +445,6 @@
             return 0
 
         lax.fori_loop(1, nz, shared_in, 0)
-    for s in near_pair:
-        send_map(s)
 
     def second(zz, _):
         for rel, core in ((0, c), (1, other)):
@@ -449,24 +464,15 @@
         extended[s, pl.ds(PAD, rows), :] = glu.astype(F32)
         rim_out[s] = glu[rows - PAD :]
 
-    def reads(s):
-        at = pl.ds(s * rows, rows)
-        raw = rounded(jnp.dot(normed[at, :], matrix(2), preferred_element_type=F32))
-        query = unit_rows(silu(raw)) * HEAD ** (-0.5)
-        scores = dot_t(query, keys_at[s]) * gammas[s]
-        read = dot(scores, solved[s])
-        base[s] = read[:, :HEAD]
-        reader[s] = (growth[s] * query - read[:, HEAD:]).astype(BF16)
-
     for s in range(NX):
         gated(s)
-    reads(0)
+    reads(far_pair[1])
 
     @pl.when(z < last)
     def _():
         remote(rim_out, rim_in, rim_sem.at[0], rim_sem.at[1], sp=z + 1).start()
 
-    for s in range(1, NX):
+    for s in near_pair:
         reads(s)
 
     @pl.when(z > 0)
@@ -499,20 +505,21 @@
     @pl.when(is_composer)
     def _():
         arrived(start, s_recv.at[0])
+        states[0] = start[...].astype(BF16)
 
         def advance(i, state):
-            states[i] = state.astype(BF16)
+            give(i)
             arrived(map_in.at[i], map_recv.at[i])
             block = map_in[i]
-            keep = block[HEAD : HEAD + 1, :HEAD].astype(F32) + block[HEAD + 8 : HEAD + 9, :HEAD].astype(F32)
+            keep = block[HEAD : HEAD + 1, :HEAD].astype(F32) + block[HEAD + 4 : HEAD + 5, :HEAD].astype(F32)
             high = state.astype(BF16)
             low = state - high.astype(F32)
             reduce = dot(block[:HEAD, HEAD:], high) + dot(block[:HEAD, HEAD:], low)
             result = keep * state - reduce + block[:HEAD, :HEAD].astype(F32)
-            give(i)
+            states[i + 1] = result.astype(BF16)
             return result
 
-        states[last] = lax.fori_loop(0, last, advance, start[...]).astype(BF16)
+        lax.fori_loop(0, last, advance, start[...])
 
     def exchange(src, dst, send, recv):
         for d in range(NX):
@@ -591,15 +598,6 @@
         return 0
 
     lax.fori_loop(0, half // 2, conv_part, 0)
-    exchanged(attn_out, attn_all, attn_send, attn_recv)
-
-    def attn_part(j, _):
-        total = partial[j] + jnp.dot(attn_all[...], weights(j, 0), preferred_element_type=F32)
-        out_ref[:, pl.ds(pl.multiple_of(j * 2 * HEAD, 2 * HEAD), 2 * HEAD)] = total.astype(BF16)
-        return 0
-
-    lax.fori_loop(0, half // 2, attn_part, 0)
-
     def drain_ring(t, _):
         for pos in range(count):
             for way in range(2):
@@ -652,13 +650,22 @@
     lax.fori_loop(0, half, drain_half, 0)
     for s in range(NX):
 
-        @pl.when((z != s * quarter + quarter // 2) & (z != last))
+        @pl.when((z != s * quarter + other * (quarter // 2)) & (z != last))
         def _(s=s):
             remote(map_out.at[s], map_in.at[z], map_send.at[s], map_recv.at[z], sp=0).wait_send()
 
     @pl.when(z < last)
     def _():
         remote(rim_out, rim_in, rim_sem.at[0], rim_sem.at[1], sp=z + 1).wait_send()
+
+    exchanged(attn_out, attn_all, attn_send, attn_recv)
+
+    def attn_part(j, _):
+        total = partial[j] + jnp.dot(attn_all[...], weights(j, 0), preferred_element_type=F32)
+        out_ref[:, pl.ds(pl.multiple_of(j * 2 * HEAD, 2 * HEAD), 2 * HEAD)] = total.astype(BF16)
+        return 0
+
+    lax.fori_loop(0, half // 2, attn_part, 0)
 
 
 def mixed_tokens(nz, paired, tokens, *rest):
@@ -689,8 +696,8 @@
             pltpu.VMEM((NX, rows, 2 * HEAD), BF16),
             pltpu.VMEM((NX, rows, HEAD), F32),
             pltpu.VMEM((NX, rows, HEAD), BF16),
-            pltpu.VMEM((NX, HEAD + 16, 2 * HEAD), BF16),
-            pltpu.VMEM((nz, HEAD + 16, 2 * HEAD), BF16),
+            pltpu.VMEM((NX, HEAD + 8, 2 * HEAD), BF16),
+            pltpu.VMEM((nz, HEAD + 8, 2 * HEAD), BF16),
             pltpu.VMEM((nz, HEAD, HEAD), BF16),
             pltpu.VMEM((NX, HEAD, HEAD), BF16),
             pltpu.VMEM((NX, PAD, HEAD), BF16),

time: 110 us -> 106 us (0.964)
  Pallas kernels: 108 us -> 104 us
    pallas_call x1, Pallas kernels: 108 us -> 104 us  [mixed_tokens(): pl.pallas_call(functools.partial(kernel, nz, paired), name='mix', out_sha...]
where the time goes in v4:
time: 106 us
  Pallas kernels  104 us (98%)
  local copies, waits for them, and re-layouts  1.87 us (2%)
    pallas_call x1, Pallas kernels, mixed_tokens(): pl.pallas_call(functools.partial(kernel, nz, paired), name='mix', out_sha...  104 us

profile of v4, /device:TPU:33, one launch (start us, length us, event | category | flops | bytes accessed | tf_op | source)
XLA Modules:
  0.0 105.6 jit_solution(3208764206209966893)
XLA Ops:
  0.0 103.7 %mix.1 = bf16[256,1024]{1,0:T(8,128)(2,1)} custom-call(bf16[256,1024]{1,0:T(8,128)(2,1)} %bitcast.12, bf16[128,512]{1,0:T(8,128)(2,1)} %k_ref.1, bf16[128,512]{1,0:T(8,128)(2,1)} %v_ref.1, bf16[128,512]{1,0:T(8,128)(2,1)} %q_ref.1, bf16[128,512]{1,0:T(8,128)(2,1)} %up_ref.1, bf16[128,512]{1,0:T(8,128)(2,1)} %gate_ref.1, bf16[512,128]{1,0:T(8,128)(2,1)} %do_ref.1, ...), custom_call_target="tpu_custom_call" | custom-call | tf_op jit(solution)/shard_map/mix/pallas_call | solution.py:679
  103.7 1.9 %copy.20 = bf16[1,256,1024]{2,1,0:T(8,128)(2,1)} copy(bf16[1,256,1024]{2,1,0:T(8,128)(2,1)} %bitcast.11) | data formatting | bytes 1048576

commit v5 on v4

--- a/solution.py
+++ b/solution.py
@@ -424,19 +424,20 @@
     here = lax.div(z, quarter)
     far_pair = [lax.rem(here + k, NX) for k in (2, 1)]
     near_pair = [lax.rem(here + k, NX) for k in (3, 0)]
-    finish(far_pair, [terms(s) for s in far_pair])
+    pending = [terms(s) for s in far_pair]
     last_hop(range(2, count))
     for i in range(len(shared)):
         to_partner(far, i).start()
+    finish(far_pair, pending)
     pending = [terms(s) for s in near_pair]
     for s in far_pair:
         send_map(s)
+    whole_piece(far)
+    spread(far)
     finish(near_pair, pending)
     reads(far_pair[0])
     for s in near_pair:
         send_map(s)
-    whole_piece(far)
-    spread(far)
     if paired:
 
         def shared_in(d, _):

time: 106 us -> 105 us (level)
  no operation moved by 1% of the time
where the time goes in v5:
time: 105 us
  Pallas kernels  103 us (98%)
  local copies, waits for them, and re-layouts  1.87 us (2%)
    pallas_call x1, Pallas kernels, mixed_tokens(): pl.pallas_call(functools.partial(kernel, nz, paired), name='mix', out_sha...  103 us

profile of v5, /device:TPU:33, one launch (start us, length us, event | category | flops | bytes accessed | tf_op | source)
XLA Modules:
  0.0 105.0 jit_solution(2239744527362541806)
XLA Ops:
  0.0 103.1 %mix.1 = bf16[256,1024]{1,0:T(8,128)(2,1)} custom-call(bf16[256,1024]{1,0:T(8,128)(2,1)} %bitcast.12, bf16[128,512]{1,0:T(8,128)(2,1)} %k_ref.1, bf16[128,512]{1,0:T(8,128)(2,1)} %v_ref.1, bf16[128,512]{1,0:T(8,128)(2,1)} %q_ref.1, bf16[128,512]{1,0:T(8,128)(2,1)} %up_ref.1, bf16[128,512]{1,0:T(8,128)(2,1)} %gate_ref.1, bf16[512,128]{1,0:T(8,128)(2,1)} %do_ref.1, ...), custom_call_target="tpu_custom_call" | custom-call | tf_op jit(solution)/shard_map/mix/pallas_call | solution.py:680
  103.1 1.9 %copy.20 = bf16[1,256,1024]{2,1,0:T(8,128)(2,1)} copy(bf16[1,256,1024]{2,1,0:T(8,128)(2,1)} %bitcast.11) | data formatting | bytes 1048576
